TPU v7x, 128 devices: a whole 4x4x4 slice. The times are simulated.
128 devices in a mesh: sp: 16 (over z, x), tp: 4 (over y), dp: 2 (over core).
Axes of the slice: x: 4, y: 4, z: 4, core: 2. Of those that a mesh axis runs over, the one named last changes fastest.
Arguments:
- latent_tokens: bfloat16 [16384, 2048], P(('dp', 'sp', 'tp')), parts along dimension 0, may hold values from -6 to 6
- condition: bfloat16 [4096], P(('dp', 'sp')), parts along dimension 0, may hold values from -6 to 6
- shift_weight: bfloat16 [2048, 2048], P('sp', 'tp'), may hold values from -0.125 to 0.125
- scale_weight: bfloat16 [2048, 2048], P('sp', 'tp'), may hold values from -0.125 to 0.125
- gate_weight: bfloat16 [2048, 2048], P('sp', 'tp'), may hold values from -0.125 to 0.125
- norm_gain: float32 [2048], replicated, may hold values from 0.1 to 1.9
- query_down: bfloat16 [2048, 512], replicated, may hold values from -0.125 to 0.125
- query_gain: float32 [512], replicated, may hold values from 0.1 to 1.9
- kv_down: bfloat16 [2048, 256], replicated, may hold values from -0.125 to 0.125
- kv_gain: float32 [256], replicated, may hold values from 0.1 to 1.9
- rope_down: bfloat16 [2048, 32], replicated, may hold values from -0.125 to 0.125
- query_up: bfloat16 [512, 1536], P(None, 'tp'), may hold values from -0.25 to 0.25
- key_up: bfloat16 [256, 1024], P(None, 'tp'), may hold values from -0.375 to 0.375
- value_up: bfloat16 [256, 1024], P(None, 'tp'), may hold values from -0.375 to 0.375
- query_norm_gain: float32 [96], replicated, may hold values from 0.47 to 16
- key_norm_gain: float32 [96], replicated, may hold values from 0.47 to 16
- out_weight: bfloat16 [1024, 2048], P('tp'), may hold values from -0.1875 to 0.1875
- context_latent: bfloat16 [2048, 256], P(('dp', 'sp')), parts along dimension 0, may hold values from -6 to 6
- context_rope: bfloat16 [2048, 32], P(('dp', 'sp')), parts along dimension 0, may hold values from -6 to 6
- context_lift: float32 [16], P('tp'), may hold values from 0 to 2
Outputs:
- output: bfloat16 [16384, 2048], P(('dp', 'sp', 'tp')), parts along dimension 0
There are 2 independent parts, one for each index of `dp`. A program takes and returns all parts, laid end to end along the dimension named above; an argument that names none is the same for every part. Nothing has to cross between parts.
All inputs are finite; a program needn't handle non-finite values.
Results may differ from a plain program's by a relative error of at most 0.015.
The roundings to bfloat16 on the way count: a program that leaves them out, or rounds other values in their place, can miss the bound.
Values may be sent and summed in bfloat16 or wider, within the bound.
A program may use at most 128 MiB of HBM per device.

v0:
```python
import jax
import jax.numpy as jnp
from jax import lax
from jax.experimental import pallas as pl
from jax.experimental.pallas import tpu as pltpu
from jax.sharding import PartitionSpec as P

NOPE_DIM = 64
ROPE_DIM = 32
VALUE_DIM = 64
QK_DIM = 96
GRID_W = 64
EPS = 1e-06
THETA = 10000.0
LOG2E = 1.4426950408889634

F32 = jnp.float32
BF16 = jnp.bfloat16
MESH = pl.DeviceIdType.MESH
VMEM = pl.BlockSpec(memory_space=pltpu.VMEM)


def send(src, dst, send_sem, recv_sem, to):
    c = pltpu.make_async_remote_copy(
        src_ref=src, dst_ref=dst, send_sem=send_sem, recv_sem=recv_sem, device_id=to, device_id_type=MESH
    )
    c.start()
    return c


def turned(rows, cosine, sine):
    out = []
    for a in range(2):
        u, w = rows[16 * a : 16 * a + 8], rows[16 * a + 8 : 16 * a + 16]
        out += [u * cosine[a] - w * sine[a], w * cosine[a] + u * sine[a]]
    return jnp.concatenate(out, axis=0)


def column(row):
    row = jnp.concatenate([row, jnp.zeros((1, 32), F32)], axis=1)
    return jnp.broadcast_to(row, (128, 128)).T[:QK_DIM]


def front_kernel(
    cond_ref, shift_ref, scale_ref, gate_ref, ng_ref, qgain_ref, kvgain_ref, qng_ref, kng_ref, freq_ref,
    x_hbm, qd_hbm, kvd_hbm, rd_hbm, qw_hbm, kw_hbm, vw_hbm, lat_hbm, rope_hbm,
    out_ref, gate_out, clat_ref, crope_ref,
    x_s, qd_s, kvd_s, rd_s, wq_s, wkv_s, near_s, near_g, wide_s, wide_g,
    s_near, r_near, s_neg, r_neg, s_wide, r_wide, s_wig, r_wig, s_lat, r_lat, s_rope, r_rope,
    s_q, r_q, s_kv, r_kv, s_qc, r_qc, s_kvc, r_kvc, local_sem,
):
    sp, tp, core = lax.axis_index("sp"), lax.axis_index("tp"), lax.axis_index("dp")
    partner = {"dp": 1 - core}

    def along_tp(k):
        return {"tp": lax.rem(tp + k, 4)}

    def along_sp(r):
        return {"sp": lax.rem(sp + r, 16)}

    barrier = pltpu.get_barrier_semaphore()
    for to in [along_tp(k) for k in range(1, 4)] + [along_sp(r) for r in range(1, 16)] + [partner]:
        pl.semaphore_signal(barrier, inc=1, device_id=to, device_id_type=MESH)
    own = []

    def fetch(src, dst):
        c = pltpu.make_async_copy(src, dst, local_sem.at[len(own)])
        c.start()
        own.append(c)

    for h in range(2):
        fetch(qw_hbm.at[256 * h : 256 * h + 256], wq_s.at[0, h])
        fetch(kw_hbm.at[128 * h : 128 * h + 128], wkv_s.at[0, h, :, 0:256])
        fetch(vw_hbm.at[128 * h : 128 * h + 128], wkv_s.at[0, h, :, 256:512])
    fetch(x_hbm, x_s)
    fetch(qd_hbm, qd_s)
    fetch(kvd_hbm, kvd_s)
    fetch(rd_hbm, rd_s)
    fetch(lat_hbm, clat_ref.at[0])
    fetch(rope_hbm, crope_ref.at[0])

    cond = cond_ref[...].astype(F32)
    active = cond / (1.0 + jnp.exp(-cond))
    active = jnp.broadcast_to(active, (16, 128)).astype(BF16)
    for i, w_ref in enumerate((shift_ref, scale_ref, gate_ref)):
        row = jnp.dot(active, w_ref[...], preferred_element_type=F32)
        for j in range(4):
            piece = row[0:1, 128 * j : 128 * j + 128]
            if i < 2:
                near_s[tp, 4 * i + j : 4 * i + j + 1, :] = piece
            else:
                near_g[tp, j : j + 1, :] = piece
    near_g[tp, 4:8, :] = jnp.zeros((4, 128), F32)
    pl.semaphore_wait(barrier, 19)

    nears, negs = [], []
    for k in range(1, 4):
        nears.append(send(near_s.at[tp], near_s.at[tp], s_near.at[k], r_near.at[k], along_tp(k)))
    for k in range(1, 4):
        negs.append(send(near_g.at[tp], near_g.at[tp], s_neg.at[k], r_neg.at[k], along_tp(k)))
    for i in range(6):
        own[i].wait()
    near_w = []
    for k in (1, 3):
        near_w.append(send(wq_s.at[0, core], wq_s.at[4 - k, core], s_q.at[k], r_q.at[k], along_tp(k)))
        near_w.append(send(wkv_s.at[0, core], wkv_s.at[4 - k, core], s_kv.at[k], r_kv.at[k], along_tp(k)))

    for c in nears:
        c.wait_recv()
    wides, wigs, rest = [], [], []
    for r in range(1, 16):
        wides.append(send(near_s, wide_s.at[r], s_wide.at[r], r_wide.at[r], along_sp(r)))
    for c in negs:
        c.wait_recv()
    for r in range(1, 16):
        wigs.append(send(near_g, wide_g.at[r], s_wig.at[r], r_wig.at[r], along_sp(r)))
    for r in range(1, 16):
        rest.append(send(lat_hbm, clat_ref.at[r], s_lat.at[r], r_lat.at[r], along_sp(r)))
        rest.append(send(rope_hbm, crope_ref.at[r], s_rope.at[r], r_rope.at[r], along_sp(r)))

    lane = lax.broadcasted_iota(jnp.int32, (8, 128), 1)
    first = (sp * 4 + tp) * 2
    angles = [
        (first + lane // GRID_W).astype(F32) * freq_ref[...],
        lax.rem(lane, GRID_W).astype(F32) * freq_ref[...],
    ]
    cosine, sine = [jnp.cos(v) for v in angles], [jnp.sin(v) for v in angles]
    q_gain = column(qng_ref[...] * (LOG2E * QK_DIM**-0.5))
    k_gain = column(kng_ref[...])
    for c in own[6:]:
        c.wait()
    values = x_s[...].astype(F32)
    mean_square = jnp.mean(values * values, axis=-1, keepdims=True)
    scaled = values * lax.rsqrt(mean_square + EPS) * ng_ref[...]

    total = near_s[...]
    for r in range(1, 16):
        wides[r - 1].wait_recv()
        total = total + wide_s[r]
    mod = [
        jnp.concatenate([total[i, 4 * k + j : 4 * k + j + 1] for i in range(4) for j in range(4)], axis=1)
        for k in range(2)
    ]
    normed = (scaled * (1.0 + mod[1]) + mod[0]).astype(BF16)

    def latent(w, gain_ref):
        y = jnp.dot(normed, w[...], preferred_element_type=F32)
        m = jnp.mean(y * y, axis=-1, keepdims=True)
        return (y * lax.rsqrt(m + EPS) * gain_ref[...]).astype(BF16)

    ql = latent(qd_s, qgain_ref)
    kl = latent(kvd_s, kvgain_ref)
    rk = lax.dot_general(rd_s[...], normed, (((1,), (1,)), ((), ())), preferred_element_type=F32)
    rk = rk.astype(BF16).astype(F32)
    rk_square = jnp.sum(rk * rk, axis=0, keepdims=True)

    shared = []

    def share(k):
        shared.append(send(wq_s.at[k, core], wq_s.at[k, core], s_qc.at[k], r_qc.at[k], partner))
        shared.append(send(wkv_s.at[k, core], wkv_s.at[k, core], s_kvc.at[k], r_kvc.at[k], partner))

    for c in near_w:
        c.wait_recv()
    far_w = [
        send(wq_s.at[3, core], wq_s.at[2, core], s_q.at[2], r_q.at[2], along_tp(1)),
        send(wkv_s.at[1, core], wkv_s.at[2, core], s_kv.at[2], r_kv.at[2], along_tp(3)),
    ]
    share(3)
    share(1)

    def expand(k):
        q = jnp.dot(ql, wq_s[k].reshape(512, 384), preferred_element_type=F32).T
        kv = jnp.dot(kl, wkv_s[k].reshape(256, 512), preferred_element_type=F32).T
        for j in range(4):
            qh = q[QK_DIM * j : QK_DIM * (j + 1)]
            inv = lax.rsqrt(jnp.sum(qh * qh, axis=0, keepdims=True) * (1.0 / QK_DIM) + EPS)
            qh = qh * inv * q_gain
            qh = jnp.concatenate([qh[:NOPE_DIM], turned(qh[NOPE_DIM:], cosine, sine)], axis=0)
            out_ref[k, j, 0:QK_DIM, :] = qh.astype(BF16)
            kh = kv[NOPE_DIM * j : NOPE_DIM * (j + 1)]
            square = jnp.sum(kh * kh, axis=0, keepdims=True) + rk_square
            inv = lax.rsqrt(square * (1.0 / QK_DIM) + EPS)
            kr = turned(rk * inv * k_gain[NOPE_DIM:], cosine, sine)
            kh = kh * inv * k_gain[:NOPE_DIM]
            out_ref[k, j, QK_DIM : QK_DIM + NOPE_DIM, :] = kh.astype(BF16)
            out_ref[k, j, QK_DIM + NOPE_DIM : 2 * QK_DIM, :] = kr.astype(BF16)
            vh = kv[256 + VALUE_DIM * j : 256 + VALUE_DIM * (j + 1)]
            out_ref[k, j, 2 * QK_DIM : 256, :] = vh.astype(BF16)

    expand(0)
    for c in shared[0:4]:
        c.wait_recv()
    expand(3)
    expand(1)
    for c in far_w:
        c.wait_recv()
    share(2)
    gates = near_g[...]
    for r in range(1, 16):
        wigs[r - 1].wait_recv()
        gates = gates + wide_g[r]
    gate_out[...] = gates
    for c in shared[4:6]:
        c.wait_recv()
    expand(2)
    for c in rest:
        c.wait()
    for c in nears + negs + near_w + wides + wigs + far_w + shared:
        c.wait_send()


def front(*args):
    dma = pltpu.SemaphoreType.DMA
    hbm = pl.BlockSpec(memory_space=pltpu.HBM)
    return pl.pallas_call(
        front_kernel,
        out_shape=(
            jax.ShapeDtypeStruct((4, 4, 256, 128), BF16),
            jax.ShapeDtypeStruct((4, 8, 128), F32),
            jax.ShapeDtypeStruct((16, 64, 256), BF16),
            jax.ShapeDtypeStruct((16, 32, 64), BF16),
        ),
        in_specs=[VMEM] * 10 + [hbm] * 9,
        out_specs=(VMEM,) * 4,
        scratch_shapes=[
            pltpu.VMEM((128, 2048), BF16),
            pltpu.VMEM((2048, 512), BF16),
            pltpu.VMEM((2048, 256), BF16),
            pltpu.VMEM((32, 2048), BF16),
            pltpu.VMEM((4, 2, 256, 384), BF16),
            pltpu.VMEM((4, 2, 128, 512), BF16),
            pltpu.VMEM((4, 8, 128), F32),
            pltpu.VMEM((4, 8, 128), F32),
            pltpu.VMEM((16, 4, 8, 128), F32),
            pltpu.VMEM((16, 4, 8, 128), F32),
            dma((4,)), dma((4,)), dma((4,)), dma((4,)),
            dma((16,)), dma((16,)), dma((16,)), dma((16,)), dma((16,)), dma((16,)), dma((16,)), dma((16,)),
            dma((4,)), dma((4,)), dma((4,)), dma((4,)), dma((4,)), dma((4,)), dma((4,)), dma((4,)),
            dma((12,)),
        ],
        compiler_params=pltpu.CompilerParams(
            collective_id=0, has_side_effects=True, vmem_limit_bytes=32 * 1024 * 1024
        ),
        cost_estimate=pl.CostEstimate(flops=800_000_000, bytes_accessed=8_000_000, transcendentals=10_000),
        name="front",
    )(*args)


CHUNK = 1536
TILE = 512
SUB = 256
STEPS = CHUNK // SUB
PLANE = [(db, dy) for dy in range(4) for db in range(4)]


def back_kernel(
    qkv_ref, clat_ref, crope_ref, kup_ref, vup_ref, kg_ref, lift_ref, x_hbm, gate_ref, wout_hbm, out_ref,
    q_in, kvs, q_s, k_s, v_s, s_s, m_s, top_s, acc_s, att_s, slots, w_s, x_s,
    s_q, r_q, s_kv, r_kv, s_up, r_up, s_down, r_down, s_far, r_far, s_att, r_att,
    s_w, r_w, s_wc, r_wc, local_sem,
):
    sp, tp, core = lax.axis_index("sp"), lax.axis_index("tp"), lax.axis_index("dp")
    z, x = sp // 4, lax.rem(sp, 4)
    a, b = z + core * (x - z), x + core * (z - x)

    def at(da, db, dy):
        aa, bb = lax.rem(a + da, 4), lax.rem(b + db, 4)
        return {"sp": aa * (4 - 3 * core) + bb * (1 + 3 * core), "tp": lax.rem(tp + dy, 4)}

    up, down, partner = at(1, 0, 0), at(3, 0, 0), {"dp": 1 - core}
    barrier = pltpu.get_barrier_semaphore()
    for to in [at(0, db, dy) for db, dy in PLANE[1:]] + [up, down, partner]:
        pl.semaphore_signal(barrier, inc=1, device_id=to, device_id_type=MESH)
    own = [
        pltpu.make_async_copy(qkv_ref.at[0, b, 0:96], q_in.at[0], local_sem.at[0]),
        pltpu.make_async_copy(qkv_ref.at[0, b, 96:256], kvs.at[0, 0], local_sem.at[1]),
        pltpu.make_async_copy(x_hbm, x_s, local_sem.at[2]),
        pltpu.make_async_copy(wout_hbm.at[0:128], w_s.at[0, 0], local_sem.at[3]),
        pltpu.make_async_copy(wout_hbm.at[128:256], w_s.at[0, 1], local_sem.at[4]),
    ]
    for c in own:
        c.start()
    pl.semaphore_wait(barrier, 18)
    q_copies, kv_copies = [None], [None]
    for r in range(1, 16):
        db, dy = PLANE[r]
        head = lax.rem(b + db, 4)
        q_copies.append(send(qkv_ref.at[dy, head, 0:96], q_in.at[r], s_q.at[r], r_q.at[r], at(0, db, dy)))
    for r in range(1, 16):
        db, dy = PLANE[r]
        head = lax.rem(b + db, 4)
        kv_copies.append(send(qkv_ref.at[dy, head, 96:256], kvs.at[0, r], s_kv.at[r], r_kv.at[r], at(0, db, dy)))

    def own_head(w_ref):
        w = w_ref[...].astype(F32)
        w = jnp.where(b < 2, w[:, :128], w[:, 128:])
        return jnp.where(lax.rem(b, 2) == 0, w, pltpu.roll(w, 64, 1)).astype(BF16)

    clat = clat_ref[...].reshape(1024, 256)
    kn = jnp.dot(clat, own_head(kup_ref), preferred_element_type=F32)
    lane = lax.broadcasted_iota(jnp.int32, (1, 128), 1)
    ropes = []
    for i in range(8):
        two = jnp.concatenate([crope_ref[2 * i], crope_ref[2 * i + 1]], axis=1).astype(F32)
        two = jnp.concatenate([jnp.zeros((64, 128), F32), two, jnp.zeros((32, 128), F32)], axis=0)
        ropes.append(two.T)
    key = jnp.where(lane < NOPE_DIM, kn, jnp.concatenate(ropes, axis=0))
    inv = lax.rsqrt(jnp.sum(key * key, axis=1, keepdims=True) * (1.0 / QK_DIM) + EPS)
    gain = jnp.concatenate([kg_ref[...], jnp.zeros((1, 32), F32)], axis=1)
    lift = jnp.full((1, 128), lift_ref[b] * LOG2E, F32)
    high = lift.astype(BF16).astype(F32)
    middle = (lift - high).astype(BF16).astype(F32)
    low = lift - high - middle
    extra = jnp.where(lane == 96, high, jnp.where(lane == 97, middle, jnp.where(lane == 98, low, 0.0)))
    k_s[0, 0:1024, :] = (key * inv * gain + extra).astype(BF16)
    vv = jnp.dot(clat, own_head(vup_ref), preferred_element_type=F32).T
    v_s[0, 0:VALUE_DIM, 0:1024] = vv[:VALUE_DIM].astype(BF16)
    for i in range(2):
        v_s[i, VALUE_DIM:80, :] = jnp.ones((16, CHUNK), BF16)
    for t in range(4):
        q_s[t, QK_DIM:128, :] = jnp.ones((32, TILE), BF16)
    m_s[...] = jnp.full(m_s.shape, -1e30, F32)
    acc_s[...] = jnp.zeros(acc_s.shape, F32)

    def place(chunk, first, blocks):
        for i, (slot, r) in enumerate(blocks):
            at_key = first + 128 * i
            block = kvs[slot, r]
            kt = jnp.concatenate([block[:QK_DIM].astype(F32), jnp.zeros((32, 128), F32)], axis=0)
            k_s[chunk % 2, at_key : at_key + 128, :] = kt.T.astype(BF16)
            v_s[chunk % 2, 0:VALUE_DIM, at_key : at_key + 128] = block[QK_DIM:]

    ups, downs, far, wides = [], [], [], []

    def spread(g):
        for r in range(max(1, 4 * g), 4 * g + 4):
            kv_copies[r].wait_recv()
        rows = pl.ds(4 * g, 4)
        ups.append(send(kvs.at[0, rows], kvs.at[1, rows], s_up.at[g], r_up.at[g], up))
        downs.append(send(kvs.at[0, rows], kvs.at[2, rows], s_down.at[g], r_down.at[g], down))

    def farther(g):
        rows = pl.ds(4 * g, 4)
        slot, to = (1, up) if g < 2 else (2, down)
        far.append(send(kvs.at[slot, rows], kvs.at[3, rows], s_far.at[g], r_far.at[g], to))

    def rows_of(slot, *groups):
        return [(slot, 4 * g + i) for g in groups for i in range(4)]

    y_up, y_down = at(0, 0, 1), at(0, 0, 3)

    def weights_near():
        own[3].wait()
        own[4].wait()
        wides.append(send(w_s.at[0, core], w_s.at[3, core], s_w.at[0], r_w.at[0], y_up))
        wides.append(send(w_s.at[0, core], w_s.at[1, core], s_w.at[1], r_w.at[1], y_down))

    wide_far, shared = [], []

    def weights_far():
        wides[0].wait_recv()
        wides[1].wait_recv()
        wide_far.append(
            send(w_s.at[3, core, 0:64], w_s.at[2, core, 0:64], s_w.at[2], r_w.at[2], y_up)
        )
        wide_far.append(
            send(w_s.at[1, core, 64:128], w_s.at[2, core, 64:128], s_w.at[3], r_w.at[3], y_down)
        )
        for k in (3, 1):
            shared.append(send(w_s.at[k, core], w_s.at[k, core], s_wc.at[k], r_wc.at[k], partner))

    def weights_share():
        for c in wide_far:
            c.wait_recv()
        shared.append(send(w_s.at[2, core], w_s.at[2, core], s_wc.at[2], r_wc.at[2], partner))

    def prepare(chunk):
        if chunk == 0:
            own[1].wait()
            spread(0)
            place(0, 1024, rows_of(0, 0))
        elif chunk == 1:
            for g in range(1, 4):
                spread(g)
            weights_near()
            place(1, 0, rows_of(0, 1, 2, 3))
        elif chunk == 2:
            for g in range(3):
                ups[g].wait_recv()
            farther(0)
            farther(1)
            place(2, 0, rows_of(1, 0, 1, 2))
        elif chunk == 3:
            for g in range(1, 4):
                downs[g].wait_recv()
            farther(2)
            farther(3)
            place(3, 0, rows_of(2, 1, 2, 3))
        elif chunk == 4:
            ups[3].wait_recv()
            downs[0].wait_recv()
            far[0].wait_recv()
            place(4, 0, rows_of(1, 3) + rows_of(2, 0) + rows_of(3, 0))
            weights_far()
        else:
            for g in range(1, 4):
                far[g].wait_recv()
            place(5, 0, rows_of(3, 1, 2, 3))

    def score(chunk, t, i):
        rows = slice(i * SUB, (i + 1) * SUB)
        s = jnp.dot(k_s[chunk % 2, rows], q_s[t], preferred_element_type=F32)
        s_s[rows] = s
        return jnp.max(s.reshape(SUB // 8, 8, TILE), axis=0)

    def step(chunk, t, later_chunk, later):
        old = m_s[t]
        new = jnp.maximum(old, jnp.max(top_s[...], axis=0, keepdims=True))
        m_s[t] = new
        acc = acc_s[t] * jnp.exp2(old - new)
        top = None
        for i in range(STEPS):
            rows = slice(i * SUB, (i + 1) * SUB)
            p = jnp.exp2(s_s[rows] - new).astype(BF16)
            acc = acc + jnp.dot(v_s[chunk % 2, :, rows], p, preferred_element_type=F32)
            if later is not None:
                part = score(later_chunk, later, i)
                top = part if top is None else jnp.maximum(top, part)
        acc_s[t] = acc
        if later is not None:
            top_s[...] = top

    att_copies = []

    def finish(t):
        acc = acc_s[t]
        o = (acc[:VALUE_DIM] / acc[VALUE_DIM : VALUE_DIM + 1]).astype(BF16)
        for i in range(4):
            att_s[4 * t + i] = o[:, 128 * i : 128 * i + 128]

    def give(t):
        for r in range(4 * t, 4 * t + 4):
            db, dy = PLANE[r]
            if r:
                att_copies.append(
                    send(
                        att_s.at[r], slots.at[dy, b], s_att.at[r], r_att.at[r],
                        at(0, (4 - db) % 4, (4 - dy) % 4),
                    )
                )
            else:
                slots[0, b] = att_s[0]

    own[0].wait()
    q_s[0, 0:QK_DIM, 0:128] = q_in[0]
    for r in range(1, 16):
        q_copies[r].wait_recv()
        q_s[r // 4, 0:QK_DIM, 128 * (r % 4) : 128 * (r % 4) + 128] = q_in[r]
    prepare(0)
    top = None
    for i in range(STEPS):
        part = score(0, 0, i)
        top = part if top is None else jnp.maximum(top, part)
    top_s[...] = top
    for chunk in range(6):
        if chunk < 5:

            def some_tile(t, carry, chunk=chunk):
                step(chunk, t, chunk, t + 1)
                return carry

            lax.fori_loop(0, 3, some_tile, 0)
            prepare(chunk + 1)
            step(chunk, 3, chunk + 1, 0)
        else:
            for t in range(4):
                step(chunk, t, chunk, t + 1 if t < 3 else None)
                finish(t)
                if t:
                    give(t - 1)
                if t == 1:
                    weights_share()
            give(3)

    own[2].wait()
    for c in shared:
        c.wait_recv()
    for c in att_copies:
        c.wait_recv()
    atts = []
    for k in range(4):
        atts.append(slots[k].reshape(256, 128).astype(F32).T.astype(BF16))
    gate = [gate_ref[i, j : j + 1, :] for i in range(4) for j in range(4)]
    for n in range(4):
        cols = slice(512 * n, 512 * n + 512)
        mixed = None
        for k in range(4):
            w = w_s[k, :, :, cols].reshape(256, 512)
            term = jnp.dot(atts[k], w, preferred_element_type=F32).astype(BF16).astype(F32)
            mixed = term if mixed is None else mixed + term
        gated = jnp.concatenate(gate[4 * n : 4 * n + 4], axis=1)
        out_ref[:, cols] = (x_s[:, cols].astype(F32) + gated * mixed).astype(BF16)
    for c in q_copies[1:] + kv_copies[1:] + ups + downs + far + wides + wide_far + shared + att_copies:
        c.wait_send()


def back(*args):
    dma = pltpu.SemaphoreType.DMA
    hbm = pl.BlockSpec(memory_space=pltpu.HBM)
    return pl.pallas_call(
        back_kernel,
        out_shape=jax.ShapeDtypeStruct((128, 2048), BF16),
        in_specs=[VMEM] * 6 + [pl.BlockSpec(memory_space=pltpu.SMEM), hbm, VMEM, hbm],
        out_specs=VMEM,
        scratch_shapes=[
            pltpu.VMEM((16, QK_DIM, 128), BF16),
            pltpu.VMEM((4, 16, 160, 128), BF16),
            pltpu.VMEM((4, 128, TILE), BF16),
            pltpu.VMEM((2, CHUNK, 128), BF16),
            pltpu.VMEM((2, 80, CHUNK), BF16),
            pltpu.VMEM((CHUNK, TILE), F32),
            pltpu.VMEM((4, 1, TILE), F32),
            pltpu.VMEM((8, TILE), F32),
            pltpu.VMEM((4, 80, TILE), F32),
            pltpu.VMEM((16, VALUE_DIM, 128), BF16),
            pltpu.VMEM((4, 4, VALUE_DIM, 128), BF16),
            pltpu.VMEM((4, 2, 128, 2048), BF16),
            pltpu.VMEM((128, 2048), BF16),
            dma((16,)), dma((16,)), dma((16,)), dma((16,)),
            dma((4,)), dma((4,)), dma((4,)), dma((4,)), dma((4,)), dma((4,)), dma((16,)), dma((16,)),
            dma((4,)), dma((4,)), dma((4,)), dma((4,)), dma((5,)),
        ],
        compiler_params=pltpu.CompilerParams(
            collective_id=1, has_side_effects=True, vmem_limit_bytes=48 * 1024 * 1024
        ),
        cost_estimate=pl.CostEstimate(
            flops=10_000_000_000, bytes_accessed=8_000_000, transcendentals=19_000_000
        ),
        name="back",
    )(*args)


def local(
    latent_tokens, condition, shift_weight, scale_weight, gate_weight, norm_gain, query_down, query_gain,
    kv_down, kv_gain, rope_down, query_up, key_up, value_up, query_norm_gain, key_norm_gain, out_weight,
    context_latent, context_rope, context_lift,
):
    frequency = THETA ** (-4.0 * jnp.arange(8, dtype=F32) / ROPE_DIM)
    qkv, gates, clat, crope = front(
        condition.reshape(1, 128), shift_weight, scale_weight, gate_weight,
        norm_gain.reshape(1, -1), query_gain.reshape(1, -1), kv_gain.reshape(1, -1),
        query_norm_gain.reshape(1, -1), key_norm_gain.reshape(1, -1),
        jnp.broadcast_to(frequency[:, None], (8, 128)),
        latent_tokens, query_down, kv_down, rope_down.T, query_up, key_up, value_up,
        context_latent, context_rope.T,
    )
    return back(
        qkv, clat, crope, key_up, value_up, key_norm_gain.reshape(1, -1), context_lift,
        latent_tokens, gates, out_weight,
    )


def solution(mesh):
    in_specs = (
        P(("dp", "sp", "tp"), None), P(("dp", "sp")), P("sp", "tp"), P("sp", "tp"), P("sp", "tp"),
        P(), P(), P(), P(), P(), P(), P(None, "tp"), P(None, "tp"), P(None, "tp"), P(), P(),
        P("tp", None), P(("dp", "sp"), None), P(("dp", "sp"), None), P("tp"),
    )
    return jax.shard_map(
        local, mesh=mesh, in_specs=in_specs, out_specs=P(("dp", "sp", "tp"), None), check_vma=False
    )
```

profile of v0, /device:TPU:0, one launch (start us, length us, event | category | flops | bytes accessed | tf_op | source)
XLA Modules:
  0.0 93.4 jit_solution(15603882748249576768)
XLA Ops:
  0.0 0.1 broadcast_in_dim.2.freq_ref
  0.1 0.0 copy-start
  0.1 1.6 %copy-done = bf16[2048,512]{1,0:T(8,128)(2,1)S(1)} copy-done((bf16[2048,512]{1,0:T(8,128)(2,1)S(1)}, bf16[2048,512]{1,0:T(8,128)(2,1)}, u32[]{:S(2)}) %copy-start) | copy-done | bytes 2097176
  1.7 0.0 copy-start.1
  1.7 1.2 %copy-done.1 = bf16[2048,256]{1,0:T(8,128)(2,1)S(1)} copy-done((bf16[2048,256]{1,0:T(8,128)(2,1)S(1)}, bf16[2048,256]{1,0:T(8,128)(2,1)}, u32[]{:S(2)}) %copy-start.1) | copy-done | bytes 1048600
  2.9 0.0 copy-start.2
  2.9 1.0 %copy-done.2 = bf16[128,2048]{1,0:T(8,128)(2,1)S(1)} copy-done((bf16[128,2048]{1,0:T(8,128)(2,1)S(1)}, bf16[128,2048]{1,0:T(8,128)(2,1)}, u32[]{:S(2)}) %copy-start.2) | copy-done | bytes 524312
  3.9 0.0 copy-start.4
  4.0 1.0 %copy-done.4 = bf16[512,384]{1,0:T(8,128)(2,1)S(1)} copy-done((bf16[512,384]{1,0:T(8,128)(2,1)S(1)}, bf16[512,384]{1,0:T(8,128)(2,1)}, u32[]{:S(2)}) %copy-start.4) | copy-done | bytes 393240
  4.9 0.0 copy-start.5
  4.9 0.9 copy-done.5
  5.8 0.0 copy-start.6
  5.9 0.9 copy-done.6
  6.8 0.0 copy-start.7
  6.8 0.9 copy-done.7
  7.7 0.0 copy-start.8
  7.7 0.9 copy-done.8
  8.6 0.0 copy-start.9
  8.6 0.9 copy-done.9
  9.5 0.0 copy-start.11
  9.5 0.9 copy-done.11
  10.4 0.0 copy-start.13
  10.4 0.8 copy-done.13
  11.1 0.0 copy-start.14
  11.1 0.7 copy-done.14
  11.8 0.0 copy-start.15
  11.8 0.7 copy-done.15
  12.5 0.0 copy-start.16
  12.5 0.7 copy-done.16
  13.2 0.0 copy-start.17
  13.2 0.7 copy-done.17
  13.9 0.0 copy-start.18
  13.9 0.7 copy-done.18
  14.5 0.0 copy-start.19
  14.5 0.7 copy-done.19
  15.2 0.0 copy-start.20
  15.2 0.7 copy-done.20
  15.9 0.0 copy-start.3
  15.9 0.0 copy-start.10
  15.9 0.0 copy-start.12
  15.9 0.0 copy-start.21
  15.9 0.0 copy-start.22
  15.9 0.0 copy-start.23
  15.9 29.8 %front.1 = (bf16[4,4,256,128]{3,2,1,0:T(8,128)(2,1)S(1)}, f32[4,8,128]{2,1,0:T(8,128)S(1)}, bf16[16,64,256]{2,1,0:T(8,128)(2,1)S(1)}, bf16[16,32,64]{2,1,0:T(8,128)(2,1)S(1)}) custom-call(bf16[1,128]{1,0:T(2,128)(2,1)S(1)} %bitcast.13, bf16[128,512]{1,0:T(8,128)(2,1)S(1)} %copy-done.5, bf16[128,512]{1,0:T(8,128)(2,1)S(1)} %copy-done.6, ...), custom_call_target="tpu_custom_call" | custom-call | flops 800000000 | bytes 8000000 | tf_op jit(solution)/shard_map/front/pallas_call | solution.py:216
  45.7 0.0 copy-done.3
  45.7 0.0 copy-done.10
  45.7 0.0 copy-done.12
  45.7 0.0 copy-done.21
  45.7 0.0 copy-done.22
  45.7 0.0 copy-done.23
  45.7 46.8 %back.1 = bf16[128,2048]{1,0:T(8,128)(2,1)S(1)} custom-call(bf16[4,4,256,128]{3,2,1,0:T(8,128)(2,1)S(1)} %get-tuple-element.9.qkv_ref, bf16[16,64,256]{2,1,0:T(8,128)(2,1)S(1)} %get-tuple-element.10.clat_ref, bf16[16,32,64]{2,1,0:T(8,128)(2,1)S(1)} %get-tuple-element.11.crope_ref, bf16[256,256]{1,0:T(8,128)(2,1)S(1)} %copy-done.10, ...), custom_call_target="tpu_custom_call" | custom-call | flops 10000000000 | bytes 8000000 | tf_op jit(solution)/shard_map/back/pallas_call | solution.py:511
  92.6 0.8 copy.22
  (1 shorter events, 0.0 us)
Async XLA Ops:
  0.1 1.6 %copy-start = (bf16[2048,512]{1,0:T(8,128)(2,1)S(1)}, bf16[2048,512]{1,0:T(8,128)(2,1)}, u32[]{:S(2)}) copy-start(bf16[2048,512]{1,0:T(8,128)(2,1)} %qd_hbm.1) | copy-start | bytes 6291460
  1.7 1.2 %copy-start.1 = (bf16[2048,256]{1,0:T(8,128)(2,1)S(1)}, bf16[2048,256]{1,0:T(8,128)(2,1)}, u32[]{:S(2)}) copy-start(bf16[2048,256]{1,0:T(8,128)(2,1)} %kvd_hbm.1) | copy-start | bytes 3145732
  2.9 1.0 %copy-start.2 = (bf16[128,2048]{1,0:T(8,128)(2,1)S(1)}, bf16[128,2048]{1,0:T(8,128)(2,1)}, u32[]{:S(2)}) copy-start(bf16[128,2048]{1,0:T(8,128)(2,1)} %x_hbm.3) | copy-start | bytes 1572868
  3.9 1.0 %copy-start.4 = (bf16[512,384]{1,0:T(8,128)(2,1)S(1)}, bf16[512,384]{1,0:T(8,128)(2,1)}, u32[]{:S(2)}) copy-start(bf16[512,384]{1,0:T(8,128)(2,1)} %qw_hbm.1) | copy-start | bytes 1179652
  4.9 0.9 copy-start.5
  5.8 0.9 copy-start.6
  6.8 0.9 copy-start.7
  7.7 0.9 copy-start.8
  8.6 0.9 copy-start.9
  9.5 0.9 copy-start.11
  10.4 0.8 copy-start.13
  11.1 0.7 copy-start.14
  11.8 0.7 copy-start.15
  12.5 0.7 copy-start.16
  13.2 0.7 copy-start.17
  13.9 0.7 copy-start.18
  14.5 0.7 copy-start.19
  15.2 0.7 copy-start.20
  15.9 29.8 %copy-start.3 = (bf16[128,2048]{1,0:T(8,128)(2,1)S(1)}, bf16[128,2048]{1,0:T(8,128)(2,1)}, u32[]{:S(2)}) copy-start(bf16[128,2048]{1,0:T(8,128)(2,1)} %x_hbm.3) | copy-start | bytes 1572868
  15.9 29.8 %copy-start.10 = (bf16[256,256]{1,0:T(8,128)(2,1)S(1)}, bf16[256,256]{1,0:T(8,128)(2,1)}, u32[]{:S(2)}) copy-start(bf16[256,256]{1,0:T(8,128)(2,1)} %kup_ref.1) | copy-start | bytes 393220
  15.9 29.8 %copy-start.12 = (bf16[256,256]{1,0:T(8,128)(2,1)S(1)}, bf16[256,256]{1,0:T(8,128)(2,1)}, u32[]{:S(2)}) copy-start(bf16[256,256]{1,0:T(8,128)(2,1)} %vup_ref.1) | copy-start | bytes 393220
  15.9 29.9 %copy-start.21 = (f32[96]{0:T(128)S(1)}, f32[96]{0:T(128)}, u32[]{:S(2)}) copy-start(f32[96]{0:T(128)} %param.35) | copy-start | bytes 1156
  15.9 29.9 %copy-start.22 = (bf16[256,2048]{1,0:T(8,128)(2,1)S(1)}, bf16[256,2048]{1,0:T(8,128)(2,1)}, u32[]{:S(2)}) copy-start(bf16[256,2048]{1,0:T(8,128)(2,1)} %wout_hbm.1) | copy-start | bytes 3145732
  15.9 29.9 %copy-start.23 = (f32[4]{0:T(128)S(1)}, f32[4]{0:T(128)}, u32[]{:S(2)}) copy-start(f32[4]{0:T(128)} %lift_ref.1) | copy-start | bytes 52
where the time goes:
time: 94 us; the launch traced here: 93.4 us
  Pallas kernels  76.6 us (81%)
  local copies, waits for them, and re-layouts  16.6 us (18%)
    pallas_call x1, Pallas kernels, back(): pl.pallas_call(back_kernel, out_shape=jax.ShapeDtypeStruct((128, 2048), B...  46.8 us
    pallas_call x1, Pallas kernels, front(): pl.pallas_call(front_kernel, out_shape=(jax.ShapeDtypeStruct((4, 4, 256,...  29.8 us
    unnamed x49, local copies, waits for them, and re-layouts  16.6 us

commit v1 on v0

v1 whole, which is shorter than its diff:
```python
import jax
import jax.numpy as jnp
from jax import lax
from jax.experimental import pallas as pl
from jax.experimental.pallas import tpu as pltpu
from jax.sharding import PartitionSpec as P

NOPE_DIM = 64
ROPE_DIM = 32
VALUE_DIM = 64
QK_DIM = 96
GRID_W = 64
EPS = 1e-06
THETA = 10000.0
LOG2E = 1.4426950408889634

F32 = jnp.float32
BF16 = jnp.bfloat16
MESH = pl.DeviceIdType.MESH
VMEM = pl.BlockSpec(memory_space=pltpu.VMEM)


CHUNK = 1536
TILE = 512
SUB = 256
STEPS = CHUNK // SUB
PIECE = (0, 3, 1, 2)
OPPOSITE = (0, 2, 1, 3)


def send(src, dst, send_sem, recv_sem, to):
    c = pltpu.make_async_remote_copy(
        src_ref=src, dst_ref=dst, send_sem=send_sem, recv_sem=recv_sem, device_id=to, device_id_type=MESH
    )
    c.start()
    return c


def dot(a, b):
    return jnp.dot(a, b, preferred_element_type=F32)


def turned(rows, cosine, sine):
    out = []
    for a in range(2):
        u, w = rows[16 * a : 16 * a + 8], rows[16 * a + 8 : 16 * a + 16]
        out += [u * cosine[a] - w * sine[a], w * cosine[a] + u * sine[a]]
    return jnp.concatenate(out, axis=0)


def column(row):
    row = jnp.concatenate([row, jnp.zeros((1, 32), F32)], axis=1)
    return jnp.broadcast_to(row, (128, 128)).T[:QK_DIM]


def kernel(
    cond_hbm, shift_hbm, scale_hbm, gate_hbm, ng_hbm, qgain_hbm, kvgain_hbm, qng_hbm, kng_hbm, freq_hbm,
    x_hbm, qd_hbm, kvd_hbm, rd_hbm, qw_hbm, kw_hbm, vw_hbm, lat_hbm, rope_hbm, wout_hbm, lift_ref,
    out_ref,
    cond_s, mw_s, ng_s, qgain_s, kvgain_s, qng_s, kng_s, freq_s,
    x_s, qd_s, kvd_s, rd_s, qw_s, kw_s, vw_s, clat_s, crope_s,
    near_s, near_g, wide_s, wide_g, gates_s, ql_s, kl_s, rk_s,
    qkv_s, q_in, kvs, q_s, k_s, v_s, s_s, m_s, top_s, acc_s, att_s, slots, w_s,
    s_near, r_near, s_neg, r_neg, s_wide, r_wide, s_wig, r_wig, s_lat, r_lat, s_rope, r_rope,
    s_ql, r_ql, s_kl, r_kl, s_rk, r_rk, s_q, r_q, s_kv, r_kv,
    s_up, r_up, s_down, r_down, s_far, r_far, s_att, r_att, s_w, r_w, s_wc, r_wc, local_sem, block_sem,
):
    sp, tp, core = lax.axis_index("sp"), lax.axis_index("tp"), lax.axis_index("dp")
    z, x = sp // 4, lax.rem(sp, 4)
    a, b = z + core * (x - z), x + core * (z - x)

    def at(da, db, dy):
        aa, bb = lax.rem(a + da, 4), lax.rem(b + db, 4)
        return {"sp": aa * (4 - 3 * core) + bb * (1 + 3 * core), "tp": lax.rem(tp + dy, 4)}

    def along_tp(k):
        return {"tp": lax.rem(tp + k, 4)}

    def along_sp(r):
        return {"sp": lax.rem(sp + r, 16)}

    partner, y_up, y_down = {"dp": 1 - core}, along_tp(1), along_tp(3)
    a_up, a_down = at(1, 0, 0), at(3, 0, 0)
    barrier = pltpu.get_barrier_semaphore()
    greeted = [along_tp(k) for k in range(1, 4)] + [along_sp(r) for r in range(1, 16)] + [partner]
    greeted += [at(0, db, dy) for dy in range(1, 4) for db in range(1, 4)]
    for to in greeted:
        pl.semaphore_signal(barrier, inc=1, device_id=to, device_id_type=MESH)
    own = []

    def fetch(src, dst):
        c = pltpu.make_async_copy(src, dst, local_sem.at[len(own)])
        c.start()
        own.append(c)

    for src, dst in (
        (cond_hbm, cond_s), (shift_hbm, mw_s.at[0]), (scale_hbm, mw_s.at[1]), (gate_hbm, mw_s.at[2]),
        (freq_hbm, freq_s), (qng_hbm, qng_s), (kng_hbm, kng_s), (x_hbm, x_s), (ng_hbm, ng_s),
        (qd_hbm, qd_s), (kvd_hbm, kvd_s), (rd_hbm, rd_s), (qgain_hbm, qgain_s), (kvgain_hbm, kvgain_s),
        (qw_hbm, qw_s), (kw_hbm, kw_s), (vw_hbm, vw_s), (lat_hbm, clat_s.at[0]), (rope_hbm, crope_s.at[0]),
        (wout_hbm.at[0:128], w_s.at[0, 0]), (wout_hbm.at[128:256], w_s.at[0, 1]),
    ):
        fetch(src, dst)

    for c in own[:4]:
        c.wait()
    cond = cond_s[...].astype(F32)
    active = cond / (1.0 + jnp.exp(-cond))
    active = jnp.broadcast_to(active, (16, 128)).astype(BF16)
    for i in range(3):
        row = dot(active, mw_s[i])
        for j in range(4):
            piece = row[0:1, 128 * j : 128 * j + 128]
            if i < 2:
                near_s[tp, 4 * i + j : 4 * i + j + 1, :] = piece
            else:
                near_g[tp, j : j + 1, :] = piece
    near_g[tp, 4:8, :] = jnp.zeros((4, 128), F32)
    pl.semaphore_wait(barrier, len(greeted))

    nears, negs = [], []
    for k in range(1, 4):
        nears.append(send(near_s.at[tp], near_s.at[tp], s_near.at[k], r_near.at[k], along_tp(k)))
    for k in range(1, 4):
        negs.append(send(near_g.at[tp], near_g.at[tp], s_neg.at[k], r_neg.at[k], along_tp(k)))

    weights = [[], []]

    def weights_near(part):
        rows, src = pl.ds(64 * part, 64), wout_hbm.at[pl.ds(core * 128 + 64 * part, 64)]
        i = 2 * part
        weights[part].append(send(src, w_s.at[1, core, rows], s_w.at[i], r_w.at[i], y_up))
        weights[part].append(send(src, w_s.at[2, core, rows], s_w.at[i + 1], r_w.at[i + 1], y_down))

    weights_near(0)

    for c in nears:
        c.wait_recv()
    wides, wigs, rest = [], [], []
    for r in range(1, 16):
        wides.append(send(near_s, wide_s.at[r], s_wide.at[r], r_wide.at[r], along_sp(r)))
    for c in negs:
        c.wait_recv()
    for r in range(1, 16):
        wigs.append(send(near_g, wide_g.at[r], s_wig.at[r], r_wig.at[r], along_sp(r)))
    for r in range(1, 16):
        rest.append(send(lat_hbm, clat_s.at[r], s_lat.at[r], r_lat.at[r], along_sp(r)))
        rest.append(send(rope_hbm, crope_s.at[r], s_rope.at[r], r_rope.at[r], along_sp(r)))

    for c in own[4:]:
        c.wait()
    lane = lax.broadcasted_iota(jnp.int32, (8, 128), 1)
    column_angle = lax.rem(lane, GRID_W).astype(F32) * freq_s[...]
    column_cosine, column_sine = jnp.cos(column_angle), jnp.sin(column_angle)
    tables = []
    for p in range(4):
        row = (sp * 4 + lax.rem(tp + PIECE[p], 4)) * 2 + lane // GRID_W
        angle = row.astype(F32) * freq_s[...]
        tables.append(((jnp.cos(angle), column_cosine), (jnp.sin(angle), column_sine)))
    q_gain = column(qng_s[...] * (LOG2E * QK_DIM**-0.5))
    k_gain = column(kng_s[...])
    for i in range(2):
        v_s[i, VALUE_DIM:80, :] = jnp.ones((16, CHUNK), BF16)
    for t in range(4):
        q_s[t, QK_DIM:128, :] = jnp.ones((32, TILE), BF16)
    m_s[...] = jnp.full(m_s.shape, -1e30, F32)
    acc_s[...] = jnp.zeros(acc_s.shape, F32)
    values = x_s[...].astype(F32)
    mean_square = jnp.mean(values * values, axis=-1, keepdims=True)
    scaled = values * lax.rsqrt(mean_square + EPS) * ng_s[...]

    total = near_s[...]
    for r in range(1, 16):
        wides[r - 1].wait_recv()
        total = total + wide_s[r]
    mod = [
        jnp.concatenate([total[i, 4 * k + j : 4 * k + j + 1] for i in range(4) for j in range(4)], axis=1)
        for k in range(2)
    ]
    normed = (scaled * (1.0 + mod[1]) + mod[0]).astype(BF16)

    def latent(w, gain_ref):
        y = dot(normed, w[...])
        m = jnp.mean(y * y, axis=-1, keepdims=True)
        return (y * lax.rsqrt(m + EPS) * gain_ref[...]).astype(BF16)

    rk = lax.dot_general(rd_s[...], normed, (((1,), (1,)), ((), ())), preferred_element_type=F32)
    rk_s[0] = rk.astype(BF16)
    kl_s[0] = latent(kvd_s, kvgain_s)
    ql_s[0] = latent(qd_s, qgain_s)
    gates = near_g[...]
    for r in range(1, 16):
        wigs[r - 1].wait_recv()
        gates = gates + wide_g[r]
    gates_s[...] = gates
    latents = [[], [], [], []]
    for p, to in ((1, y_up), (2, y_down)):
        latents[p].append(send(kl_s.at[0], kl_s.at[p], s_kl.at[p], r_kl.at[p], to))
        latents[p].append(send(rk_s.at[0], rk_s.at[p], s_rk.at[p], r_rk.at[p], to))
        latents[p].append(send(ql_s.at[0], ql_s.at[p], s_ql.at[p], r_ql.at[p], to))

    q_copies, kv_copies, own_kv = {}, {}, []

    def expand(p):
        for c in latents[p]:
            c.wait_recv()
        if p == 2:
            latents[3].append(send(ql_s.at[1], ql_s.at[3], s_ql.at[3], r_ql.at[3], y_up))
            latents[3].append(send(kl_s.at[2], kl_s.at[3], s_kl.at[3], r_kl.at[3], y_down))
            latents[3].append(send(rk_s.at[2], rk_s.at[3], s_rk.at[3], r_rk.at[3], y_down))
            weights_near(1)
        cosine, sine = tables[p]
        rk = rk_s[p].astype(F32)
        rk_square = jnp.sum(rk * rk, axis=0, keepdims=True)
        q, kn, vv = dot(ql_s[p], qw_s[...]).T, dot(kl_s[p], kw_s[...]).T, dot(kl_s[p], vw_s[...]).T
        for j in range(4):
            qh = q[QK_DIM * j : QK_DIM * (j + 1)]
            inv = lax.rsqrt(jnp.sum(qh * qh, axis=0, keepdims=True) * (1.0 / QK_DIM) + EPS)
            qh = qh * inv * q_gain
            qh = jnp.concatenate([qh[:NOPE_DIM], turned(qh[NOPE_DIM:], cosine, sine)], axis=0)
            qkv_s[p, j, 0:QK_DIM, :] = qh.astype(BF16)
            kh = kn[NOPE_DIM * j : NOPE_DIM * (j + 1)]
            square = jnp.sum(kh * kh, axis=0, keepdims=True) + rk_square
            inv = lax.rsqrt(square * (1.0 / QK_DIM) + EPS)
            kr = turned(rk * inv * k_gain[NOPE_DIM:], cosine, sine)
            kh = kh * inv * k_gain[:NOPE_DIM]
            qkv_s[p, j, QK_DIM : QK_DIM + NOPE_DIM, :] = kh.astype(BF16)
            qkv_s[p, j, QK_DIM + NOPE_DIM : 2 * QK_DIM, :] = kr.astype(BF16)
            qkv_s[p, j, 2 * QK_DIM : 256, :] = vv[VALUE_DIM * j : VALUE_DIM * (j + 1)].astype(BF16)
        c = pltpu.make_async_copy(qkv_s.at[p, b, QK_DIM:256], kvs.at[0, 4 * p], block_sem.at[p])
        c.start()
        own_kv.append(c)
        for db in range(1, 4):
            r, block = 4 * p + db, qkv_s.at[p, lax.rem(b + db, 4)]
            q_copies[r] = send(block.at[0:QK_DIM], q_in.at[r], s_q.at[r], r_q.at[r], at(0, db, 0))
        for db in range(1, 4):
            r, block = 4 * p + db, qkv_s.at[p, lax.rem(b + db, 4)]
            kv_copies[r] = send(block.at[QK_DIM:256], kvs.at[0, r], s_kv.at[r], r_kv.at[r], at(0, db, 0))

    expand(0)

    def own_head(w_ref):
        w = w_ref[...].astype(F32)
        w = jnp.where(b < 2, w[:, :128], w[:, 128:])
        return jnp.where(lax.rem(b, 2) == 0, w, pltpu.roll(w, 64, 1)).astype(BF16)

    for c in rest:
        c.wait_recv()
    clat = clat_s[...].reshape(1024, 256)
    kn = dot(clat, own_head(kw_s))
    lane = lax.broadcasted_iota(jnp.int32, (1, 128), 1)
    ropes = []
    for i in range(8):
        two = jnp.concatenate([crope_s[2 * i], crope_s[2 * i + 1]], axis=1).astype(F32)
        two = jnp.concatenate([jnp.zeros((64, 128), F32), two, jnp.zeros((32, 128), F32)], axis=0)
        ropes.append(two.T)
    key = jnp.where(lane < NOPE_DIM, kn, jnp.concatenate(ropes, axis=0))
    inv = lax.rsqrt(jnp.sum(key * key, axis=1, keepdims=True) * (1.0 / QK_DIM) + EPS)
    gain = jnp.concatenate([kng_s[...], jnp.zeros((1, 32), F32)], axis=1)
    lift = jnp.full((1, 128), lift_ref[b] * LOG2E, F32)
    high = lift.astype(BF16).astype(F32)
    middle = (lift - high).astype(BF16).astype(F32)
    low = lift - high - middle
    extra = jnp.where(lane == 96, high, jnp.where(lane == 97, middle, jnp.where(lane == 98, low, 0.0)))
    k_s[0, 0:1024, :] = (key * inv * gain + extra).astype(BF16)
    vv = dot(clat, own_head(vw_s)).T
    v_s[0, 0:VALUE_DIM, 0:1024] = vv[:VALUE_DIM].astype(BF16)

    def place(chunk, first, blocks):
        for i, (slot, r) in enumerate(blocks):
            at_key = first + 128 * i
            block = kvs[slot, r]
            kt = jnp.concatenate([block[:QK_DIM].astype(F32), jnp.zeros((32, 128), F32)], axis=0)
            k_s[chunk % 2, at_key : at_key + 128, :] = kt.T.astype(BF16)
            v_s[chunk % 2, 0:VALUE_DIM, at_key : at_key + 128] = block[QK_DIM:]

    def take_queries(p):
        q_s[p, 0:QK_DIM, 0:128] = qkv_s[p, b, 0:QK_DIM]
        for db in range(1, 4):
            q_copies[4 * p + db].wait_recv()
            q_s[p, 0:QK_DIM, 128 * db : 128 * db + 128] = q_in[4 * p + db]

    ups, downs, far = [], [], []

    def spread(g):
        own_kv[g].wait()
        for db in range(1, 4):
            kv_copies[4 * g + db].wait_recv()
        rows = pl.ds(4 * g, 4)
        ups.append(send(kvs.at[0, rows], kvs.at[1, rows], s_up.at[g], r_up.at[g], a_up))
        downs.append(send(kvs.at[0, rows], kvs.at[2, rows], s_down.at[g], r_down.at[g], a_down))

    def farther(g):
        rows = pl.ds(4 * g, 4)
        slot, to = (1, a_up) if g < 2 else (2, a_down)
        far.append(send(kvs.at[slot, rows], kvs.at[3, rows], s_far.at[g], r_far.at[g], to))

    def rows_of(slot, *groups):
        return [(slot, 4 * g + i) for g in groups for i in range(4)]

    weights_far, shared = [], []

    def forward_weights(part):
        for c in weights[part]:
            c.wait_recv()
        rows = pl.ds(64 * part, 64)
        to = y_down if part else y_up
        weights_far.append(
            send(w_s.at[1 + part, core, rows], w_s.at[3, core, rows], s_w.at[4 + part], r_w.at[4 + part], to)
        )

    def share_weights(k):
        shared.append(send(w_s.at[k, core], w_s.at[k, core], s_wc.at[k], r_wc.at[k], partner))

    def prepare(chunk):
        if chunk == 0:
            spread(0)
            place(0, 1024, rows_of(0, 0))
        elif chunk == 1:
            for g in range(1, 4):
                spread(g)
            place(1, 0, rows_of(0, 1, 2, 3))
        elif chunk == 2:
            for g in range(3):
                ups[g].wait_recv()
            farther(0)
            farther(1)
            place(2, 0, rows_of(1, 0, 1, 2))
        elif chunk == 3:
            for g in range(1, 4):
                downs[g].wait_recv()
            farther(2)
            farther(3)
            place(3, 0, rows_of(2, 1, 2, 3))
        elif chunk == 4:
            ups[3].wait_recv()
            downs[0].wait_recv()
            far[0].wait_recv()
            place(4, 0, rows_of(1, 3) + rows_of(2, 0) + rows_of(3, 0))
            forward_weights(1)
            share_weights(1)
            share_weights(2)
        else:
            for g in range(1, 4):
                far[g].wait_recv()
            place(5, 0, rows_of(3, 1, 2, 3))

    def score(chunk, t, i):
        rows = slice(i * SUB, (i + 1) * SUB)
        s = dot(k_s[chunk % 2, rows], q_s[t])
        s_s[rows] = s
        return jnp.max(s.reshape(SUB // 8, 8, TILE), axis=0)

    def step(chunk, t, later_chunk, later):
        old = m_s[t]
        new = jnp.maximum(old, jnp.max(top_s[...], axis=0, keepdims=True))
        m_s[t] = new
        acc = acc_s[t] * jnp.exp2(old - new)
        top = None
        for i in range(STEPS):
            rows = slice(i * SUB, (i + 1) * SUB)
            p = jnp.exp2(s_s[rows] - new).astype(BF16)
            acc = acc + dot(v_s[chunk % 2, :, rows], p)
            if later is not None:
                part = score(later_chunk, later, i)
                top = part if top is None else jnp.maximum(top, part)
        acc_s[t] = acc
        if later is not None:
            top_s[...] = top

    att_copies = []

    def finish(t):
        acc = acc_s[t]
        o = (acc[:VALUE_DIM] / acc[VALUE_DIM : VALUE_DIM + 1]).astype(BF16)
        for i in range(4):
            att_s[4 * t + i] = o[:, 128 * i : 128 * i + 128]

    def give(p):
        for db in range(4):
            r = 4 * p + db
            if r:
                att_copies.append(
                    send(
                        att_s.at[r], slots.at[OPPOSITE[p], b], s_att.at[r], r_att.at[r],
                        at(0, (4 - db) % 4, PIECE[p]),
                    )
                )
            else:
                slots[0, b] = att_s[0]

    expand(1)
    expand(2)
    take_queries(0)
    prepare(0)
    top = None
    for i in range(STEPS):
        part = score(0, 0, i)
        top = part if top is None else jnp.maximum(top, part)
    top_s[...] = top
    take_queries(1)
    step(0, 0, 0, 1)
    expand(3)
    forward_weights(0)
    take_queries(2)
    step(0, 1, 0, 2)
    take_queries(3)
    step(0, 2, 0, 3)
    prepare(1)
    step(0, 3, 1, 0)
    for chunk in range(1, 6):
        if chunk < 5:

            def some_tile(t, carry, chunk=chunk):
                step(chunk, t, chunk, t + 1)
                return carry

            lax.fori_loop(0, 3, some_tile, 0)
            prepare(chunk + 1)
            step(chunk, 3, chunk + 1, 0)
        else:
            for t in range(4):
                step(chunk, t, chunk, t + 1 if t < 3 else None)
                finish(t)
                if t:
                    give(t - 1)
                if t == 1:
                    for c in weights_far:
                        c.wait_recv()
                    share_weights(3)
            give(3)

    for c in shared + att_copies:
        c.wait_recv()
    atts = [slots[k].reshape(256, 128).astype(F32).T.astype(BF16) for k in range(4)]
    gate = [gates_s[i, j : j + 1, :] for i in range(4) for j in range(4)]
    for n in range(4):
        cols = slice(512 * n, 512 * n + 512)
        mixed = None
        for k in range(4):
            term = dot(atts[k], w_s[k, :, :, cols].reshape(256, 512)).astype(BF16).astype(F32)
            mixed = term if mixed is None else mixed + term
        gated = jnp.concatenate(gate[4 * n : 4 * n + 4], axis=1)
        out_ref[:, cols] = (x_s[:, cols].astype(F32) + gated * mixed).astype(BF16)
    sent = nears + negs + wides + wigs + rest + list(q_copies.values()) + list(kv_copies.values())
    sent += ups + downs + far + weights[0] + weights[1] + weights_far + shared + att_copies
    for group in latents:
        sent += group
    for c in sent:
        c.wait_send()


def everything(*args):
    dma, vmem = pltpu.SemaphoreType.DMA, pltpu.VMEM
    hbm = pl.BlockSpec(memory_space=pltpu.HBM)
    return pl.pallas_call(
        kernel,
        out_shape=jax.ShapeDtypeStruct((128, 2048), BF16),
        in_specs=[hbm] * 20 + [pl.BlockSpec(memory_space=pltpu.SMEM)],
        out_specs=VMEM,
        scratch_shapes=[
            vmem((1, 128), BF16), vmem((3, 128, 512), BF16), vmem((1, 2048), F32), vmem((1, 512), F32),
            vmem((1, 256), F32), vmem((1, 96), F32), vmem((1, 96), F32), vmem((8, 128), F32),
            vmem((128, 2048), BF16), vmem((2048, 512), BF16), vmem((2048, 256), BF16), vmem((32, 2048), BF16),
            vmem((512, 384), BF16), vmem((256, 256), BF16), vmem((256, 256), BF16),
            vmem((16, 64, 256), BF16), vmem((16, 32, 64), BF16),
            vmem((4, 8, 128), F32), vmem((4, 8, 128), F32),
            vmem((16, 4, 8, 128), F32), vmem((16, 4, 8, 128), F32), vmem((4, 8, 128), F32),
            vmem((4, 128, 512), BF16), vmem((4, 128, 256), BF16), vmem((4, 32, 128), BF16),
            vmem((4, 4, 256, 128), BF16), vmem((16, QK_DIM, 128), BF16), vmem((4, 16, 160, 128), BF16),
            vmem((4, 128, TILE), BF16), vmem((2, CHUNK, 128), BF16), vmem((2, 80, CHUNK), BF16),
            vmem((CHUNK, TILE), F32), vmem((4, 1, TILE), F32), vmem((8, TILE), F32), vmem((4, 80, TILE), F32),
            vmem((16, VALUE_DIM, 128), BF16), vmem((4, 4, VALUE_DIM, 128), BF16), vmem((4, 2, 128, 2048), BF16),
            dma((4,)), dma((4,)), dma((4,)), dma((4,)),
            dma((16,)), dma((16,)), dma((16,)), dma((16,)), dma((16,)), dma((16,)), dma((16,)), dma((16,)),
            dma((4,)), dma((4,)), dma((4,)), dma((4,)), dma((4,)), dma((4,)),
            dma((16,)), dma((16,)), dma((16,)), dma((16,)),
            dma((4,)), dma((4,)), dma((4,)), dma((4,)), dma((4,)), dma((4,)), dma((16,)), dma((16,)),
            dma((6,)), dma((6,)), dma((4,)), dma((4,)), dma((21,)), dma((4,)),
        ],
        compiler_params=pltpu.CompilerParams(
            collective_id=0, has_side_effects=True, vmem_limit_bytes=67_043_328
        ),
        cost_estimate=pl.CostEstimate(
            flops=10_000_000_000, bytes_accessed=8_000_000, transcendentals=19_000_000
        ),
        name="everything",
    )(*args)


def local(
    latent_tokens, condition, shift_weight, scale_weight, gate_weight, norm_gain, query_down, query_gain,
    kv_down, kv_gain, rope_down, query_up, key_up, value_up, query_norm_gain, key_norm_gain, out_weight,
    context_latent, context_rope, context_lift,
):
    frequency = THETA ** (-4.0 * jnp.arange(8, dtype=F32) / ROPE_DIM)
    return everything(
        condition.reshape(1, 128), shift_weight, scale_weight, gate_weight,
        norm_gain.reshape(1, -1), query_gain.reshape(1, -1), kv_gain.reshape(1, -1),
        query_norm_gain.reshape(1, -1), key_norm_gain.reshape(1, -1),
        jnp.broadcast_to(frequency[:, None], (8, 128)),
        latent_tokens, query_down, kv_down, rope_down.T, query_up, key_up, value_up,
        context_latent, context_rope.T, out_weight, context_lift,
    )


def solution(mesh):
    in_specs = (
        P(("dp", "sp", "tp"), None), P(("dp", "sp")), P("sp", "tp"), P("sp", "tp"), P("sp", "tp"),
        P(), P(), P(), P(), P(), P(), P(None, "tp"), P(None, "tp"), P(None, "tp"), P(), P(),
        P("tp", None), P(("dp", "sp"), None), P(("dp", "sp"), None), P("tp"),
    )
    return jax.shard_map(
        local, mesh=mesh, in_specs=in_specs, out_specs=P(("dp", "sp", "tp"), None), check_vma=False
    )
```

time: 94 us -> 75 us (0.80)
  local copies, waits for them, and re-layouts: 16.6 us -> 2.55 us
  Pallas kernels: 76.6 us -> 72.3 us
    unnamed x49 -> x1, local copies, waits for them, and re-layouts: 16.6 us -> 1.88 us
    pallas_call x2 -> x1, Pallas kernels: 76.6 us -> 72.3 us  [everything(): pl.pallas_call(kernel, out_shape=jax.ShapeDtypeStruct((128, 2048), BF16),...]
where the time goes in v1:
time: 75 us; the launch traced here: 74.9 us
  Pallas kernels  72.3 us (96%)
  local copies, waits for them, and re-layouts  2.55 us (3%)
    pallas_call x1, Pallas kernels, everything(): pl.pallas_call(kernel, out_shape=jax.ShapeDtypeStruct((128, 2048), BF16),...  72.3 us
    unnamed x1, local copies, waits for them, and re-layouts  1.88 us

profile of v1, /device:TPU:0, one launch (start us, length us, event | category | flops | bytes accessed | tf_op | source)
XLA Modules:
  0.0 74.9 jit_solution(5609488579935070800)
XLA Ops:
  0.0 0.7 broadcast_in_dim.2.freq_hbm
  0.7 72.3 %everything.1 = bf16[128,2048]{1,0:T(8,128)(2,1)} custom-call(bf16[1,128]{1,0:T(2,128)(2,1)} %bitcast.13, bf16[128,512]{1,0:T(8,128)(2,1)} %shift_hbm.1, bf16[128,512]{1,0:T(8,128)(2,1)} %scale_hbm.1, bf16[128,512]{1,0:T(8,128)(2,1)} %gate_hbm.1, f32[1,2048]{1,0:T(1,128)} %bitcast.9, f32[1,512]{1,0:T(1,128)} %bitcast.11, f32[1,256]{1,0:T(1,128)} %bitcast.12, ...), custom_call_target="tpu_custom_call" | custom-call | flops 10000000000 | bytes 8000000 | tf_op jit(solution)/shard_map/everything/pallas_call | solution.py:456
  73.0 1.9 %copy.22 = bf16[128,2048]{1,0:T(8,128)(2,1)} copy(bf16[128,2048]{1,0:T(8,128)(2,1)} %everything.1) | data formatting | bytes 1048576
  (1 shorter events, 0.0 us)

commit v2 on v1

--- a/solution.py
+++ b/solution.py
@@ -59,9 +59,9 @@
     out_ref,
     cond_s, mw_s, ng_s, qgain_s, kvgain_s, qng_s, kng_s, freq_s,
     x_s, qd_s, kvd_s, rd_s, qw_s, kw_s, vw_s, clat_s, crope_s,
-    near_s, near_g, wide_s, wide_g, gates_s, ql_s, kl_s, rk_s,
+    part_s, wide_s, mods_s, ql_s, kl_s, rk_s,
     qkv_s, q_in, kvs, q_s, k_s, v_s, s_s, m_s, top_s, acc_s, att_s, slots, w_s,
-    s_near, r_near, s_neg, r_neg, s_wide, r_wide, s_wig, r_wig, s_lat, r_lat, s_rope, r_rope,
+    s_near, r_near, s_wide, r_wide, s_lat, r_lat, s_rope, r_rope,
     s_ql, r_ql, s_kl, r_kl, s_rk, r_rk, s_q, r_q, s_kv, r_kv,
     s_up, r_up, s_down, r_down, s_far, r_far, s_att, r_att, s_w, r_w, s_wc, r_wc, local_sem, block_sem,
 ):
@@ -111,18 +111,23 @@
         row = dot(active, mw_s[i])
         for j in range(4):
             piece = row[0:1, 128 * j : 128 * j + 128]
-            if i < 2:
-                near_s[tp, 4 * i + j : 4 * i + j + 1, :] = piece
-            else:
-                near_g[tp, j : j + 1, :] = piece
-    near_g[tp, 4:8, :] = jnp.zeros((4, 128), F32)
+            part_s[4 * i + j : 4 * i + j + 1, :] = piece
+    part_s[12:16, :] = jnp.zeros((4, 128), F32)
     pl.semaphore_wait(barrier, len(greeted))
 
-    nears, negs = [], []
+    wides, nears, rest = [], [], []
+    for r in range(1, 16):
+        wides.append(send(part_s, wide_s.at[r], s_wide.at[r], r_wide.at[r], along_sp(r)))
+    for r in range(1, 16):
+        rest.append(send(lat_hbm, clat_s.at[r], s_lat.at[r], r_lat.at[r], along_sp(r)))
+        rest.append(send(rope_hbm, crope_s.at[r], s_rope.at[r], r_rope.at[r], along_sp(r)))
+    total = part_s[...]
+    for r in range(1, 16):
+        wides[r - 1].wait_recv()
+        total = total + wide_s[r]
+    mods_s[tp] = total
     for k in range(1, 4):
-        nears.append(send(near_s.at[tp], near_s.at[tp], s_near.at[k], r_near.at[k], along_tp(k)))
-    for k in range(1, 4):
-        negs.append(send(near_g.at[tp], near_g.at[tp], s_neg.at[k], r_neg.at[k], along_tp(k)))
+        nears.append(send(mods_s.at[tp], mods_s.at[tp], s_near.at[k], r_near.at[k], along_tp(k)))
 
     weights = [[], []]
 
@@ -131,21 +136,6 @@
         i = 2 * part
         weights[part].append(send(src, w_s.at[1, core, rows], s_w.at[i], r_w.at[i], y_up))
         weights[part].append(send(src, w_s.at[2, core, rows], s_w.at[i + 1], r_w.at[i + 1], y_down))
-
-    weights_near(0)
-
-    for c in nears:
-        c.wait_recv()
-    wides, wigs, rest = [], [], []
-    for r in range(1, 16):
-        wides.append(send(near_s, wide_s.at[r], s_wide.at[r], r_wide.at[r], along_sp(r)))
-    for c in negs:
-        c.wait_recv()
-    for r in range(1, 16):
-        wigs.append(send(near_g, wide_g.at[r], s_wig.at[r], r_wig.at[r], along_sp(r)))
-    for r in range(1, 16):
-        rest.append(send(lat_hbm, clat_s.at[r], s_lat.at[r], r_lat.at[r], along_sp(r)))
-        rest.append(send(rope_hbm, crope_s.at[r], s_rope.at[r], r_rope.at[r], along_sp(r)))
 
     for c in own[4:]:
         c.wait()
@@ -169,15 +159,13 @@
     mean_square = jnp.mean(values * values, axis=-1, keepdims=True)
     scaled = values * lax.rsqrt(mean_square + EPS) * ng_s[...]
 
-    total = near_s[...]
-    for r in range(1, 16):
-        wides[r - 1].wait_recv()
-        total = total + wide_s[r]
-    mod = [
-        jnp.concatenate([total[i, 4 * k + j : 4 * k + j + 1] for i in range(4) for j in range(4)], axis=1)
+    for c in nears:
+        c.wait_recv()
+    shift, scale = [
+        jnp.concatenate([mods_s[i, j : j + 1, :] for i in range(4) for j in range(4 * k, 4 * k + 4)], axis=1)
         for k in range(2)
     ]
-    normed = (scaled * (1.0 + mod[1]) + mod[0]).astype(BF16)
+    normed = (scaled * (1.0 + scale) + shift).astype(BF16)
 
     def latent(w, gain_ref):
         y = dot(normed, w[...])
@@ -188,11 +176,6 @@
     rk_s[0] = rk.astype(BF16)
     kl_s[0] = latent(kvd_s, kvgain_s)
     ql_s[0] = latent(qd_s, qgain_s)
-    gates = near_g[...]
-    for r in range(1, 16):
-        wigs[r - 1].wait_recv()
-        gates = gates + wide_g[r]
-    gates_s[...] = gates
     latents = [[], [], [], []]
     for p, to in ((1, y_up), (2, y_down)):
         latents[p].append(send(kl_s.at[0], kl_s.at[p], s_kl.at[p], r_kl.at[p], to))
@@ -202,13 +185,8 @@
     q_copies, kv_copies, own_kv = {}, {}, []
 
     def expand(p):
-        for c in latents[p]:
+        for c in latents[p][2:] if p == 2 else latents[p][:2] if p == 1 else latents[p]:
             c.wait_recv()
-        if p == 2:
-            latents[3].append(send(ql_s.at[1], ql_s.at[3], s_ql.at[3], r_ql.at[3], y_up))
-            latents[3].append(send(kl_s.at[2], kl_s.at[3], s_kl.at[3], r_kl.at[3], y_down))
-            latents[3].append(send(rk_s.at[2], rk_s.at[3], s_rk.at[3], r_rk.at[3], y_down))
-            weights_near(1)
         cosine, sine = tables[p]
         rk = rk_s[p].astype(F32)
         rk_square = jnp.sum(rk * rk, axis=0, keepdims=True)
@@ -237,8 +215,130 @@
             r, block = 4 * p + db, qkv_s.at[p, lax.rem(b + db, 4)]
             kv_copies[r] = send(block.at[QK_DIM:256], kvs.at[0, r], s_kv.at[r], r_kv.at[r], at(0, db, 0))
 
+    def place(chunk, first, blocks):
+        for i, (slot, r) in enumerate(blocks):
+            at_key = first + 128 * i
+            block = kvs[slot, r]
+            kt = jnp.concatenate([block[:QK_DIM].astype(F32), jnp.zeros((32, 128), F32)], axis=0)
+            k_s[chunk % 2, at_key : at_key + 128, :] = kt.T.astype(BF16)
+            v_s[chunk % 2, 0:VALUE_DIM, at_key : at_key + 128] = block[QK_DIM:]
+
+    def take_queries(p):
+        q_s[p, 0:QK_DIM, 0:128] = qkv_s[p, b, 0:QK_DIM]
+        for db in range(1, 4):
+            q_copies[4 * p + db].wait_recv()
+            q_s[p, 0:QK_DIM, 128 * db : 128 * db + 128] = q_in[4 * p + db]
+
+    ups, downs, far = {}, {}, {}
+
+    def spread(g):
+        own_kv[g].wait()
+        for db in range(1, 4):
+            kv_copies[4 * g + db].wait_recv()
+        rows = pl.ds(4 * g, 4)
+        ups[g] = send(kvs.at[0, rows], kvs.at[1, rows], s_up.at[g], r_up.at[g], a_up)
+        downs[g] = send(kvs.at[0, rows], kvs.at[2, rows], s_down.at[g], r_down.at[g], a_down)
+
+    def near(slot, g):
+        (ups if slot == 1 else downs)[g].wait_recv()
+        if (g < 2) == (slot == 1):
+            rows, to = pl.ds(4 * g, 4), a_up if slot == 1 else a_down
+            far[g] = send(kvs.at[slot, rows], kvs.at[3, rows], s_far.at[g], r_far.at[g], to)
+
+    def rows_of(slot, *groups):
+        return [(slot, 4 * g + i) for g in groups for i in range(4)]
+
+    weights_far, shared = [], []
+
+    def forward_weights(part):
+        for c in weights[part]:
+            c.wait_recv()
+        rows = pl.ds(64 * part, 64)
+        to = y_down if part else y_up
+        weights_far.append(
+            send(w_s.at[1 + part, core, rows], w_s.at[3, core, rows], s_w.at[4 + part], r_w.at[4 + part], to)
+        )
+
+    def share_weights(k):
+        shared.append(send(w_s.at[k, core], w_s.at[k, core], s_wc.at[k], r_wc.at[k], partner))
+
+    def prepare(chunk):
+        if chunk == 0:
+            spread(0)
+            place(0, 1024, rows_of(0, 0))
+        elif chunk == 1:
+            near(1, 0)
+            spread(3)
+            place(1, 0, rows_of(0, 1, 2) + rows_of(1, 0))
+        elif chunk == 2:
+            near(1, 1)
+            near(2, 2)
+            near(2, 0)
+            place(2, 0, rows_of(2, 0) + rows_of(0, 3) + rows_of(1, 1))
+            forward_weights(0)
+        elif chunk == 3:
+            near(2, 3)
+            near(1, 2)
+            near(2, 1)
+            place(3, 0, rows_of(2, 1, 2) + rows_of(1, 2))
+        elif chunk == 4:
+            near(1, 3)
+            far[0].wait_recv()
+            far[1].wait_recv()
+            place(4, 0, rows_of(3, 0, 1) + rows_of(1, 3))
+            forward_weights(1)
+            share_weights(1)
+            share_weights(2)
+        else:
+            far[2].wait_recv()
+            far[3].wait_recv()
+            place(5, 0, rows_of(3, 2, 3) + rows_of(2, 3))
+
+    def score(chunk, t, i):
+        rows = slice(i * SUB, (i + 1) * SUB)
+        s = dot(k_s[chunk % 2, rows], q_s[t])
+        s_s[rows] = s
+        return jnp.max(s.reshape(SUB // 8, 8, TILE), axis=0)
+
+    def step(chunk, t, later_chunk, later):
+        old = m_s[t]
+        new = jnp.maximum(old, jnp.max(top_s[...], axis=0, keepdims=True))
+        m_s[t] = new
+        acc = acc_s[t] * jnp.exp2(old - new)
+        top = None
+        for i in range(STEPS):
+            rows = slice(i * SUB, (i + 1) * SUB)
+            p = jnp.exp2(s_s[rows] - new).astype(BF16)
+            acc = acc + dot(v_s[chunk % 2, :, rows], p)
+            if later is not None:
+                part = score(later_chunk, later, i)
+                top = part if top is None else jnp.maximum(top, part)
+        acc_s[t] = acc
+        if later is not None:
+            top_s[...] = top
+
+    att_copies = []
+
+    def finish(t):
+        acc = acc_s[t]
+        o = (acc[:VALUE_DIM] / acc[VALUE_DIM : VALUE_DIM + 1]).astype(BF16)
+        for i in range(4):
+            att_s[4 * t + i] = o[:, 128 * i : 128 * i + 128]
+
+    def give(p):
+        for db in range(4):
+            r = 4 * p + db
+            if r:
+                att_copies.append(
+                    send(
+                        att_s.at[r], slots.at[OPPOSITE[p], b], s_att.at[r], r_att.at[r],
+                        at(0, (4 - db) % 4, PIECE[p]),
+                    )
+                )
+            else:
+                slots[0, b] = att_s[0]
+
     expand(0)
-
     def own_head(w_ref):
         w = w_ref[...].astype(F32)
         w = jnp.where(b < 2, w[:, :128], w[:, 128:])
@@ -266,129 +366,14 @@
     vv = dot(clat, own_head(vw_s)).T
     v_s[0, 0:VALUE_DIM, 0:1024] = vv[:VALUE_DIM].astype(BF16)
 
-    def place(chunk, first, blocks):
-        for i, (slot, r) in enumerate(blocks):
-            at_key = first + 128 * i
-            block = kvs[slot, r]
-            kt = jnp.concatenate([block[:QK_DIM].astype(F32), jnp.zeros((32, 128), F32)], axis=0)
-            k_s[chunk % 2, at_key : at_key + 128, :] = kt.T.astype(BF16)
-            v_s[chunk % 2, 0:VALUE_DIM, at_key : at_key + 128] = block[QK_DIM:]
-
-    def take_queries(p):
-        q_s[p, 0:QK_DIM, 0:128] = qkv_s[p, b, 0:QK_DIM]
-        for db in range(1, 4):
-            q_copies[4 * p + db].wait_recv()
-            q_s[p, 0:QK_DIM, 128 * db : 128 * db + 128] = q_in[4 * p + db]
-
-    ups, downs, far = [], [], []
-
-    def spread(g):
-        own_kv[g].wait()
-        for db in range(1, 4):
-            kv_copies[4 * g + db].wait_recv()
-        rows = pl.ds(4 * g, 4)
-        ups.append(send(kvs.at[0, rows], kvs.at[1, rows], s_up.at[g], r_up.at[g], a_up))
-        downs.append(send(kvs.at[0, rows], kvs.at[2, rows], s_down.at[g], r_down.at[g], a_down))
-
-    def farther(g):
-        rows = pl.ds(4 * g, 4)
-        slot, to = (1, a_up) if g < 2 else (2, a_down)
-        far.append(send(kvs.at[slot, rows], kvs.at[3, rows], s_far.at[g], r_far.at[g], to))
-
-    def rows_of(slot, *groups):
-        return [(slot, 4 * g + i) for g in groups for i in range(4)]
-
-    weights_far, shared = [], []
-
-    def forward_weights(part):
-        for c in weights[part]:
-            c.wait_recv()
-        rows = pl.ds(64 * part, 64)
-        to = y_down if part else y_up
-        weights_far.append(
-            send(w_s.at[1 + part, core, rows], w_s.at[3, core, rows], s_w.at[4 + part], r_w.at[4 + part], to)
-        )
-
-    def share_weights(k):
-        shared.append(send(w_s.at[k, core], w_s.at[k, core], s_wc.at[k], r_wc.at[k], partner))
-
-    def prepare(chunk):
-        if chunk == 0:
-            spread(0)
-            place(0, 1024, rows_of(0, 0))
-        elif chunk == 1:
-            for g in range(1, 4):
-                spread(g)
-            place(1, 0, rows_of(0, 1, 2, 3))
-        elif chunk == 2:
-            for g in range(3):
-                ups[g].wait_recv()
-            farther(0)
-            farther(1)
-            place(2, 0, rows_of(1, 0, 1, 2))
-        elif chunk == 3:
-            for g in range(1, 4):
-                downs[g].wait_recv()
-            farther(2)
-            farther(3)
-            place(3, 0, rows_of(2, 1, 2, 3))
-        elif chunk == 4:
-            ups[3].wait_recv()
-            downs[0].wait_recv()
-            far[0].wait_recv()
-            place(4, 0, rows_of(1, 3) + rows_of(2, 0) + rows_of(3, 0))
-            forward_weights(1)
-            share_weights(1)
-            share_weights(2)
-        else:
-            for g in range(1, 4):
-                far[g].wait_recv()
-            place(5, 0, rows_of(3, 1, 2, 3))
-
-    def score(chunk, t, i):
-        rows = slice(i * SUB, (i + 1) * SUB)
-        s = dot(k_s[chunk % 2, rows], q_s[t])
-        s_s[rows] = s
-        return jnp.max(s.reshape(SUB // 8, 8, TILE), axis=0)
-
-    def step(chunk, t, later_chunk, later):
-        old = m_s[t]
-        new = jnp.maximum(old, jnp.max(top_s[...], axis=0, keepdims=True))
-        m_s[t] = new
-        acc = acc_s[t] * jnp.exp2(old - new)
-        top = None
-        for i in range(STEPS):
-            rows = slice(i * SUB, (i + 1) * SUB)
-            p = jnp.exp2(s_s[rows] - new).astype(BF16)
-            acc = acc + dot(v_s[chunk % 2, :, rows], p)
-            if later is not None:
-                part = score(later_chunk, later, i)
-                top = part if top is None else jnp.maximum(top, part)
-        acc_s[t] = acc
-        if later is not None:
-            top_s[...] = top
-
-    att_copies = []
-
-    def finish(t):
-        acc = acc_s[t]
-        o = (acc[:VALUE_DIM] / acc[VALUE_DIM : VALUE_DIM + 1]).astype(BF16)
-        for i in range(4):
-            att_s[4 * t + i] = o[:, 128 * i : 128 * i + 128]
-
-    def give(p):
-        for db in range(4):
-            r = 4 * p + db
-            if r:
-                att_copies.append(
-                    send(
-                        att_s.at[r], slots.at[OPPOSITE[p], b], s_att.at[r], r_att.at[r],
-                        at(0, (4 - db) % 4, PIECE[p]),
-                    )
-                )
-            else:
-                slots[0, b] = att_s[0]
-
+    for c in latents[2][:2]:
+        c.wait_recv()
+    latents[3].append(send(kl_s.at[2], kl_s.at[3], s_kl.at[3], r_kl.at[3], y_down))
+    latents[3].append(send(rk_s.at[2], rk_s.at[3], s_rk.at[3], r_rk.at[3], y_down))
+    latents[1][2].wait_recv()
+    latents[3].append(send(ql_s.at[1], ql_s.at[3], s_ql.at[3], r_ql.at[3], y_up))
+    weights_near(0)
+    weights_near(1)
     expand(1)
     expand(2)
     take_queries(0)
@@ -399,9 +384,10 @@
         top = part if top is None else jnp.maximum(top, part)
     top_s[...] = top
     take_queries(1)
+    expand(3)
     step(0, 0, 0, 1)
-    expand(3)
-    forward_weights(0)
+    spread(1)
+    spread(2)
     take_queries(2)
     step(0, 1, 0, 2)
     take_queries(3)
@@ -433,7 +419,7 @@
     for c in shared + att_copies:
         c.wait_recv()
     atts = [slots[k].reshape(256, 128).astype(F32).T.astype(BF16) for k in range(4)]
-    gate = [gates_s[i, j : j + 1, :] for i in range(4) for j in range(4)]
+    gate = [mods_s[i, j : j + 1, :] for i in range(4) for j in range(8, 12)]
     for n in range(4):
         cols = slice(512 * n, 512 * n + 512)
         mixed = None
@@ -442,8 +428,8 @@
             mixed = term if mixed is None else mixed + term
         gated = jnp.concatenate(gate[4 * n : 4 * n + 4], axis=1)
         out_ref[:, cols] = (x_s[:, cols].astype(F32) + gated * mixed).astype(BF16)
-    sent = nears + negs + wides + wigs + rest + list(q_copies.values()) + list(kv_copies.values())
-    sent += ups + downs + far + weights[0] + weights[1] + weights_far + shared + att_copies
+    sent = nears + wides + rest + list(q_copies.values()) + list(kv_copies.values())
+    sent += list(ups.values()) + list(downs.values()) + list(far.values()) + weights[0] + weights[1] + weights_far + shared + att_copies
     for group in latents:
         sent += group
     for c in sent:
@@ -464,15 +450,13 @@
             vmem((128, 2048), BF16), vmem((2048, 512), BF16), vmem((2048, 256), BF16), vmem((32, 2048), BF16),
             vmem((512, 384), BF16), vmem((256, 256), BF16), vmem((256, 256), BF16),
             vmem((16, 64, 256), BF16), vmem((16, 32, 64), BF16),
-            vmem((4, 8, 128), F32), vmem((4, 8, 128), F32),
-            vmem((16, 4, 8, 128), F32), vmem((16, 4, 8, 128), F32), vmem((4, 8, 128), F32),
+            vmem((16, 128), F32), vmem((16, 16, 128), F32), vmem((4, 16, 128), F32),
             vmem((4, 128, 512), BF16), vmem((4, 128, 256), BF16), vmem((4, 32, 128), BF16),
             vmem((4, 4, 256, 128), BF16), vmem((16, QK_DIM, 128), BF16), vmem((4, 16, 160, 128), BF16),
             vmem((4, 128, TILE), BF16), vmem((2, CHUNK, 128), BF16), vmem((2, 80, CHUNK), BF16),
             vmem((CHUNK, TILE), F32), vmem((4, 1, TILE), F32), vmem((8, TILE), F32), vmem((4, 80, TILE), F32),
             vmem((16, VALUE_DIM, 128), BF16), vmem((4, 4, VALUE_DIM, 128), BF16), vmem((4, 2, 128, 2048), BF16),
-            dma((4,)), dma((4,)), dma((4,)), dma((4,)),
-            dma((16,)), dma((16,)), dma((16,)), dma((16,)), dma((16,)), dma((16,)), dma((16,)), dma((16,)),
+            dma((4,)), dma((4,)), dma((16,)), dma((16,)), dma((16,)), dma((16,)), dma((16,)), dma((16,)),
             dma((4,)), dma((4,)), dma((4,)), dma((4,)), dma((4,)), dma((4,)),
             dma((16,)), dma((16,)), dma((16,)), dma((16,)),
             dma((4,)), dma((4,)), dma((4,)), dma((4,)), dma((4,)), dma((4,)), dma((16,)), dma((16,)),

time: 75 us -> 71.7 us (0.956)
  Pallas kernels: 72.3 us -> 69 us
    pallas_call x1, Pallas kernels: 72.3 us -> 69 us  [everything(): pl.pallas_call(kernel, out_shape=jax.ShapeDtypeStruct((128, 2048), BF16),...]
where the time goes in v2:
time: 71.7 us; the launch traced here: 71.6 us
  Pallas kernels  69 us (96%)
  local copies, waits for them, and re-layouts  2.55 us (4%)
    pallas_call x1, Pallas kernels, everything(): pl.pallas_call(kernel, out_shape=jax.ShapeDtypeStruct((128, 2048), BF16),...  69 us
    unnamed x1, local copies, waits for them, and re-layouts  1.88 us

profile of v2, /device:TPU:0, one launch (start us, length us, event | category | flops | bytes accessed | tf_op | source)
XLA Modules:
  0.0 71.6 jit_solution(17961149168261230469)
XLA Ops:
  0.0 0.7 broadcast_in_dim.2.freq_hbm
  0.7 69.0 %everything.1 = bf16[128,2048]{1,0:T(8,128)(2,1)} custom-call(bf16[1,128]{1,0:T(2,128)(2,1)} %bitcast.13, bf16[128,512]{1,0:T(8,128)(2,1)} %shift_hbm.1, bf16[128,512]{1,0:T(8,128)(2,1)} %scale_hbm.1, bf16[128,512]{1,0:T(8,128)(2,1)} %gate_hbm.1, f32[1,2048]{1,0:T(1,128)} %bitcast.9, f32[1,512]{1,0:T(1,128)} %bitcast.11, f32[1,256]{1,0:T(1,128)} %bitcast.12, ...), custom_call_target="tpu_custom_call" | custom-call | flops 10000000000 | bytes 8000000 | tf_op jit(solution)/shard_map/everything/pallas_call | solution.py:442
  69.7 1.9 %copy.22 = bf16[128,2048]{1,0:T(8,128)(2,1)} copy(bf16[128,2048]{1,0:T(8,128)(2,1)} %everything.1) | data formatting | bytes 1048576
  (1 shorter events, 0.0 us)

commit v3 on v2

--- a/solution.py
+++ b/solution.py
@@ -54,13 +54,13 @@
 
 
 def kernel(
-    cond_hbm, shift_hbm, scale_hbm, gate_hbm, ng_hbm, qgain_hbm, kvgain_hbm, qng_hbm, kng_hbm, freq_hbm,
+    cond_hbm, shift_hbm, scale_hbm, gate_hbm, ng_hbm, qgain_hbm, kvgain_hbm, qng_hbm, kng_hbm,
     x_hbm, qd_hbm, kvd_hbm, rd_hbm, qw_hbm, kw_hbm, vw_hbm, lat_hbm, rope_hbm, wout_hbm, lift_ref,
     out_ref,
-    cond_s, mw_s, ng_s, qgain_s, kvgain_s, qng_s, kng_s, freq_s,
+    cond_s, mw_s, ng_s, qgain_s, kvgain_s, qng_s, kng_s,
     x_s, qd_s, kvd_s, rd_s, qw_s, kw_s, vw_s, clat_s, crope_s,
     part_s, wide_s, mods_s, ql_s, kl_s, rk_s,
-    qkv_s, q_in, kvs, q_s, k_s, v_s, s_s, m_s, top_s, acc_s, att_s, slots, w_s,
+    qkv_s, q_in, kvs, q_s, k_s, v_s, s_s, m_s, top_s, acc_s, att_s, slots, w_s, mixed_s,
     s_near, r_near, s_wide, r_wide, s_lat, r_lat, s_rope, r_rope,
     s_ql, r_ql, s_kl, r_kl, s_rk, r_rk, s_q, r_q, s_kv, r_kv,
     s_up, r_up, s_down, r_down, s_far, r_far, s_att, r_att, s_w, r_w, s_wc, r_wc, local_sem, block_sem,
@@ -95,7 +95,7 @@
 
     for src, dst in (
         (cond_hbm, cond_s), (shift_hbm, mw_s.at[0]), (scale_hbm, mw_s.at[1]), (gate_hbm, mw_s.at[2]),
-        (freq_hbm, freq_s), (qng_hbm, qng_s), (kng_hbm, kng_s), (x_hbm, x_s), (ng_hbm, ng_s),
+        (qng_hbm, qng_s), (kng_hbm, kng_s), (x_hbm, x_s), (ng_hbm, ng_s),
         (qd_hbm, qd_s), (kvd_hbm, kvd_s), (rd_hbm, rd_s), (qgain_hbm, qgain_s), (kvgain_hbm, kvgain_s),
         (qw_hbm, qw_s), (kw_hbm, kw_s), (vw_hbm, vw_s), (lat_hbm, clat_s.at[0]), (rope_hbm, crope_s.at[0]),
         (wout_hbm.at[0:128], w_s.at[0, 0]), (wout_hbm.at[128:256], w_s.at[0, 1]),
@@ -115,6 +115,26 @@
     part_s[12:16, :] = jnp.zeros((4, 128), F32)
     pl.semaphore_wait(barrier, len(greeted))
 
+    weights = [[], []]
+
+    def weights_near(part):
+        rows, src = pl.ds(64 * part, 64), wout_hbm.at[pl.ds(core * 128 + 64 * part, 64)]
+        i = 2 * part
+        weights[part].append(send(src, w_s.at[1, core, rows], s_w.at[i], r_w.at[i], y_up))
+        weights[part].append(send(src, w_s.at[2, core, rows], s_w.at[i + 1], r_w.at[i + 1], y_down))
+
+    weights_far, shared = [], {}
+
+    def forward_weights(part):
+        for c in weights[part]:
+            c.wait_recv()
+        rows = pl.ds(64 * part, 64)
+        to = y_down if part else y_up
+        weights_far.append(
+            send(w_s.at[1 + part, core, rows], w_s.at[3, core, rows], s_w.at[4 + part], r_w.at[4 + part], to)
+        )
+
+    weights_near(0)
     wides, nears, rest = [], [], []
     for r in range(1, 16):
         wides.append(send(part_s, wide_s.at[r], s_wide.at[r], r_wide.at[r], along_sp(r)))
@@ -129,27 +149,23 @@
     for k in range(1, 4):
         nears.append(send(mods_s.at[tp], mods_s.at[tp], s_near.at[k], r_near.at[k], along_tp(k)))
 
-    weights = [[], []]
-
-    def weights_near(part):
-        rows, src = pl.ds(64 * part, 64), wout_hbm.at[pl.ds(core * 128 + 64 * part, 64)]
-        i = 2 * part
-        weights[part].append(send(src, w_s.at[1, core, rows], s_w.at[i], r_w.at[i], y_up))
-        weights[part].append(send(src, w_s.at[2, core, rows], s_w.at[i + 1], r_w.at[i + 1], y_down))
-
     for c in own[4:]:
         c.wait()
     lane = lax.broadcasted_iota(jnp.int32, (8, 128), 1)
-    column_angle = lax.rem(lane, GRID_W).astype(F32) * freq_s[...]
+    which = lax.broadcasted_iota(jnp.int32, (8, 128), 0)
+    frequency = jnp.full((8, 128), 1.0, F32)
+    for f in range(1, 8):
+        frequency = jnp.where(which == f, THETA ** (-4.0 * f / ROPE_DIM), frequency)
+    column_angle = lax.rem(lane, GRID_W).astype(F32) * frequency
     column_cosine, column_sine = jnp.cos(column_angle), jnp.sin(column_angle)
     tables = []
     for p in range(4):
         row = (sp * 4 + lax.rem(tp + PIECE[p], 4)) * 2 + lane // GRID_W
-        angle = row.astype(F32) * freq_s[...]
+        angle = row.astype(F32) * frequency
         tables.append(((jnp.cos(angle), column_cosine), (jnp.sin(angle), column_sine)))
     q_gain = column(qng_s[...] * (LOG2E * QK_DIM**-0.5))
     k_gain = column(kng_s[...])
-    for i in range(2):
+    for i in range(3):
         v_s[i, VALUE_DIM:80, :] = jnp.ones((16, CHUNK), BF16)
     for t in range(4):
         q_s[t, QK_DIM:128, :] = jnp.ones((32, TILE), BF16)
@@ -220,8 +236,8 @@
             at_key = first + 128 * i
             block = kvs[slot, r]
             kt = jnp.concatenate([block[:QK_DIM].astype(F32), jnp.zeros((32, 128), F32)], axis=0)
-            k_s[chunk % 2, at_key : at_key + 128, :] = kt.T.astype(BF16)
-            v_s[chunk % 2, 0:VALUE_DIM, at_key : at_key + 128] = block[QK_DIM:]
+            k_s[chunk % 3, at_key : at_key + 128, :] = kt.T.astype(BF16)
+            v_s[chunk % 3, 0:VALUE_DIM, at_key : at_key + 128] = block[QK_DIM:]
 
     def take_queries(p):
         q_s[p, 0:QK_DIM, 0:128] = qkv_s[p, b, 0:QK_DIM]
@@ -248,19 +264,8 @@
     def rows_of(slot, *groups):
         return [(slot, 4 * g + i) for g in groups for i in range(4)]
 
-    weights_far, shared = [], []
-
-    def forward_weights(part):
-        for c in weights[part]:
-            c.wait_recv()
-        rows = pl.ds(64 * part, 64)
-        to = y_down if part else y_up
-        weights_far.append(
-            send(w_s.at[1 + part, core, rows], w_s.at[3, core, rows], s_w.at[4 + part], r_w.at[4 + part], to)
-        )
-
     def share_weights(k):
-        shared.append(send(w_s.at[k, core], w_s.at[k, core], s_wc.at[k], r_wc.at[k], partner))
+        shared[k] = send(w_s.at[k, core], w_s.at[k, core], s_wc.at[k], r_wc.at[k], partner)
 
     def prepare(chunk):
         if chunk == 0:
@@ -268,35 +273,36 @@
             place(0, 1024, rows_of(0, 0))
         elif chunk == 1:
             near(1, 0)
-            spread(3)
             place(1, 0, rows_of(0, 1, 2) + rows_of(1, 0))
         elif chunk == 2:
             near(1, 1)
             near(2, 2)
             near(2, 0)
             place(2, 0, rows_of(2, 0) + rows_of(0, 3) + rows_of(1, 1))
-            forward_weights(0)
         elif chunk == 3:
             near(2, 3)
             near(1, 2)
             near(2, 1)
             place(3, 0, rows_of(2, 1, 2) + rows_of(1, 2))
+            forward_weights(1)
+            share_weights(1)
+            share_weights(2)
         elif chunk == 4:
             near(1, 3)
             far[0].wait_recv()
             far[1].wait_recv()
             place(4, 0, rows_of(3, 0, 1) + rows_of(1, 3))
-            forward_weights(1)
-            share_weights(1)
-            share_weights(2)
         else:
             far[2].wait_recv()
             far[3].wait_recv()
             place(5, 0, rows_of(3, 2, 3) + rows_of(2, 3))
+            for c in weights_far:
+                c.wait_recv()
+            share_weights(3)
 
     def score(chunk, t, i):
         rows = slice(i * SUB, (i + 1) * SUB)
-        s = dot(k_s[chunk % 2, rows], q_s[t])
+        s = dot(k_s[chunk % 3, rows], q_s[t])
         s_s[rows] = s
         return jnp.max(s.reshape(SUB // 8, 8, TILE), axis=0)
 
@@ -309,7 +315,7 @@
         for i in range(STEPS):
             rows = slice(i * SUB, (i + 1) * SUB)
             p = jnp.exp2(s_s[rows] - new).astype(BF16)
-            acc = acc + dot(v_s[chunk % 2, :, rows], p)
+            acc = acc + dot(v_s[chunk % 3, :, rows], p)
             if later is not None:
                 part = score(later_chunk, later, i)
                 top = part if top is None else jnp.maximum(top, part)
@@ -317,7 +323,7 @@
         if later is not None:
             top_s[...] = top
 
-    att_copies = []
+    att_copies = {}
 
     def finish(t):
         acc = acc_s[t]
@@ -329,11 +335,9 @@
         for db in range(4):
             r = 4 * p + db
             if r:
-                att_copies.append(
-                    send(
-                        att_s.at[r], slots.at[OPPOSITE[p], b], s_att.at[r], r_att.at[r],
-                        at(0, (4 - db) % 4, PIECE[p]),
-                    )
+                att_copies[r] = send(
+                    att_s.at[r], slots.at[OPPOSITE[p], b], s_att.at[r], r_att.at[r],
+                    at(0, (4 - db) % 4, PIECE[p]),
                 )
             else:
                 slots[0, b] = att_s[0]
@@ -372,8 +376,8 @@
     latents[3].append(send(rk_s.at[2], rk_s.at[3], s_rk.at[3], r_rk.at[3], y_down))
     latents[1][2].wait_recv()
     latents[3].append(send(ql_s.at[1], ql_s.at[3], s_ql.at[3], r_ql.at[3], y_up))
-    weights_near(0)
     weights_near(1)
+    forward_weights(0)
     expand(1)
     expand(2)
     take_queries(0)
@@ -390,11 +394,17 @@
     spread(2)
     take_queries(2)
     step(0, 1, 0, 2)
+    prepare(1)
+    step(0, 2, 1, 0)
+    step(1, 0, 1, 1)
+    step(1, 1, 1, 2)
     take_queries(3)
-    step(0, 2, 0, 3)
-    prepare(1)
-    step(0, 3, 1, 0)
-    for chunk in range(1, 6):
+    spread(3)
+    step(1, 2, 0, 3)
+    step(0, 3, 1, 3)
+    prepare(2)
+    step(1, 3, 2, 0)
+    for chunk in range(2, 6):
         if chunk < 5:
 
             def some_tile(t, carry, chunk=chunk):
@@ -410,26 +420,28 @@
                 finish(t)
                 if t:
                     give(t - 1)
-                if t == 1:
-                    for c in weights_far:
-                        c.wait_recv()
-                    share_weights(3)
             give(3)
 
-    for c in shared + att_copies:
-        c.wait_recv()
-    atts = [slots[k].reshape(256, 128).astype(F32).T.astype(BF16) for k in range(4)]
     gate = [mods_s[i, j : j + 1, :] for i in range(4) for j in range(8, 12)]
-    for n in range(4):
-        cols = slice(512 * n, 512 * n + 512)
-        mixed = None
-        for k in range(4):
-            term = dot(atts[k], w_s[k, :, :, cols].reshape(256, 512)).astype(BF16).astype(F32)
-            mixed = term if mixed is None else mixed + term
-        gated = jnp.concatenate(gate[4 * n : 4 * n + 4], axis=1)
-        out_ref[:, cols] = (x_s[:, cols].astype(F32) + gated * mixed).astype(BF16)
+    for p in range(4):
+        k = OPPOSITE[p]
+        for r in range(max(1, 4 * p), 4 * p + 4):
+            att_copies[r].wait_recv()
+        if p:
+            shared[k].wait_recv()
+        att = slots[k].reshape(256, 128).astype(F32).T.astype(BF16)
+        for n in range(4):
+            cols = slice(512 * n, 512 * n + 512)
+            term = dot(att, w_s[k, :, :, cols].reshape(256, 512)).astype(BF16).astype(F32)
+            if p:
+                term = mixed_s[:, cols] + term
+            if p < 3:
+                mixed_s[:, cols] = term
+            else:
+                gated = jnp.concatenate(gate[4 * n : 4 * n + 4], axis=1)
+                out_ref[:, cols] = (x_s[:, cols].astype(F32) + gated * term).astype(BF16)
     sent = nears + wides + rest + list(q_copies.values()) + list(kv_copies.values())
-    sent += list(ups.values()) + list(downs.values()) + list(far.values()) + weights[0] + weights[1] + weights_far + shared + att_copies
+    sent += list(ups.values()) + list(downs.values()) + list(far.values()) + weights[0] + weights[1] + weights_far + list(shared.values()) + list(att_copies.values())
     for group in latents:
         sent += group
     for c in sent:
@@ -442,20 +454,21 @@
     return pl.pallas_call(
         kernel,
         out_shape=jax.ShapeDtypeStruct((128, 2048), BF16),
-        in_specs=[hbm] * 20 + [pl.BlockSpec(memory_space=pltpu.SMEM)],
+        in_specs=[hbm] * 19 + [pl.BlockSpec(memory_space=pltpu.SMEM)],
         out_specs=VMEM,
         scratch_shapes=[
             vmem((1, 128), BF16), vmem((3, 128, 512), BF16), vmem((1, 2048), F32), vmem((1, 512), F32),
-            vmem((1, 256), F32), vmem((1, 96), F32), vmem((1, 96), F32), vmem((8, 128), F32),
+            vmem((1, 256), F32), vmem((1, 96), F32), vmem((1, 96), F32),
             vmem((128, 2048), BF16), vmem((2048, 512), BF16), vmem((2048, 256), BF16), vmem((32, 2048), BF16),
             vmem((512, 384), BF16), vmem((256, 256), BF16), vmem((256, 256), BF16),
             vmem((16, 64, 256), BF16), vmem((16, 32, 64), BF16),
             vmem((16, 128), F32), vmem((16, 16, 128), F32), vmem((4, 16, 128), F32),
             vmem((4, 128, 512), BF16), vmem((4, 128, 256), BF16), vmem((4, 32, 128), BF16),
             vmem((4, 4, 256, 128), BF16), vmem((16, QK_DIM, 128), BF16), vmem((4, 16, 160, 128), BF16),
-            vmem((4, 128, TILE), BF16), vmem((2, CHUNK, 128), BF16), vmem((2, 80, CHUNK), BF16),
+            vmem((4, 128, TILE), BF16), vmem((3, CHUNK, 128), BF16), vmem((3, 80, CHUNK), BF16),
             vmem((CHUNK, TILE), F32), vmem((4, 1, TILE), F32), vmem((8, TILE), F32), vmem((4, 80, TILE), F32),
             vmem((16, VALUE_DIM, 128), BF16), vmem((4, 4, VALUE_DIM, 128), BF16), vmem((4, 2, 128, 2048), BF16),
+            vmem((128, 2048), F32),
             dma((4,)), dma((4,)), dma((16,)), dma((16,)), dma((16,)), dma((16,)), dma((16,)), dma((16,)),
             dma((4,)), dma((4,)), dma((4,)), dma((4,)), dma((4,)), dma((4,)),
             dma((16,)), dma((16,)), dma((16,)), dma((16,)),
@@ -477,12 +490,10 @@
     kv_down, kv_gain, rope_down, query_up, key_up, value_up, query_norm_gain, key_norm_gain, out_weight,
     context_latent, context_rope, context_lift,
 ):
-    frequency = THETA ** (-4.0 * jnp.arange(8, dtype=F32) / ROPE_DIM)
     return everything(
         condition.reshape(1, 128), shift_weight, scale_weight, gate_weight,
         norm_gain.reshape(1, -1), query_gain.reshape(1, -1), kv_gain.reshape(1, -1),
         query_norm_gain.reshape(1, -1), key_norm_gain.reshape(1, -1),
-        jnp.broadcast_to(frequency[:, None], (8, 128)),
         latent_tokens, query_down, kv_down, rope_down.T, query_up, key_up, value_up,
         context_latent, context_rope.T, out_weight, context_lift,
     )

time: 71.7 us -> 68.4 us (0.954)
  Pallas kernels: 69 us -> 66.3 us
    pallas_call x1, Pallas kernels: 69 us -> 66.3 us  [everything(): pl.pallas_call(kernel, out_shape=jax.ShapeDtypeStruct((128, 2048), BF16),...]
where the time goes in v3:
time: 68.4 us; the launch traced here: 68.2 us
  Pallas kernels  66.3 us (97%)
  local copies, waits for them, and re-layouts  1.88 us (3%)
    pallas_call x1, Pallas kernels, everything(): pl.pallas_call(kernel, out_shape=jax.ShapeDtypeStruct((128, 2048), BF16),...  66.3 us
    unnamed x1, local copies, waits for them, and re-layouts  1.88 us

profile of v3, /device:TPU:0, one launch (start us, length us, event | category | flops | bytes accessed | tf_op | source)
XLA Modules:
  0.0 68.2 jit_solution(5111130228907118672)
XLA Ops:
  0.0 66.3 %everything.1 = bf16[128,2048]{1,0:T(8,128)(2,1)} custom-call(bf16[1,128]{1,0:T(2,128)(2,1)} %bitcast.13, bf16[128,512]{1,0:T(8,128)(2,1)} %shift_hbm.1, bf16[128,512]{1,0:T(8,128)(2,1)} %scale_hbm.1, bf16[128,512]{1,0:T(8,128)(2,1)} %gate_hbm.1, f32[1,2048]{1,0:T(1,128)} %bitcast.9, f32[1,512]{1,0:T(1,128)} %bitcast.11, f32[1,256]{1,0:T(1,128)} %bitcast.12, ...), custom_call_target="tpu_custom_call" | custom-call | flops 10000000000 | bytes 8000000 | tf_op jit(solution)/shard_map/everything/pallas_call | solution.py:454
  66.3 1.9 %copy.22 = bf16[128,2048]{1,0:T(8,128)(2,1)} copy(bf16[128,2048]{1,0:T(8,128)(2,1)} %everything.1) | data formatting | bytes 1048576

commit v4 on v3

--- a/solution.py
+++ b/solution.py
@@ -138,9 +138,6 @@
     wides, nears, rest = [], [], []
     for r in range(1, 16):
         wides.append(send(part_s, wide_s.at[r], s_wide.at[r], r_wide.at[r], along_sp(r)))
-    for r in range(1, 16):
-        rest.append(send(lat_hbm, clat_s.at[r], s_lat.at[r], r_lat.at[r], along_sp(r)))
-        rest.append(send(rope_hbm, crope_s.at[r], s_rope.at[r], r_rope.at[r], along_sp(r)))
     total = part_s[...]
     for r in range(1, 16):
         wides[r - 1].wait_recv()
@@ -148,6 +145,9 @@
     mods_s[tp] = total
     for k in range(1, 4):
         nears.append(send(mods_s.at[tp], mods_s.at[tp], s_near.at[k], r_near.at[k], along_tp(k)))
+    for r in range(1, 16):
+        rest.append(send(lat_hbm, clat_s.at[r], s_lat.at[r], r_lat.at[r], along_sp(r)))
+        rest.append(send(rope_hbm, crope_s.at[r], s_rope.at[r], r_rope.at[r], along_sp(r)))
 
     for c in own[4:]:
         c.wait()

time: 68.4 us -> 63.5 us (0.928)
  Pallas kernels: 66.3 us -> 61.5 us
    pallas_call x1, Pallas kernels: 66.3 us -> 61.5 us  [everything(): pl.pallas_call(kernel, out_shape=jax.ShapeDtypeStruct((128, 2048), BF16),...]
where the time goes in v4:
time: 63.5 us; the launch traced here: 63.4 us
  Pallas kernels  61.5 us (97%)
  local copies, waits for them, and re-layouts  1.88 us (3%)
    pallas_call x1, Pallas kernels, everything(): pl.pallas_call(kernel, out_shape=jax.ShapeDtypeStruct((128, 2048), BF16),...  61.5 us
    unnamed x1, local copies, waits for them, and re-layouts  1.88 us

profile of v4, /device:TPU:0, one launch (start us, length us, event | category | flops | bytes accessed | tf_op | source)
XLA Modules:
  0.0 63.4 jit_solution(16602440718242628832)
XLA Ops:
  0.0 61.5 %everything.1 = bf16[128,2048]{1,0:T(8,128)(2,1)} custom-call(bf16[1,128]{1,0:T(2,128)(2,1)} %bitcast.13, bf16[128,512]{1,0:T(8,128)(2,1)} %shift_hbm.1, bf16[128,512]{1,0:T(8,128)(2,1)} %scale_hbm.1, bf16[128,512]{1,0:T(8,128)(2,1)} %gate_hbm.1, f32[1,2048]{1,0:T(1,128)} %bitcast.9, f32[1,512]{1,0:T(1,128)} %bitcast.11, f32[1,256]{1,0:T(1,128)} %bitcast.12, ...), custom_call_target="tpu_custom_call" | custom-call | flops 10000000000 | bytes 8000000 | tf_op jit(solution)/shard_map/everything/pallas_call | solution.py:454
  61.5 1.9 %copy.22 = bf16[128,2048]{1,0:T(8,128)(2,1)} copy(bf16[128,2048]{1,0:T(8,128)(2,1)} %everything.1) | data formatting | bytes 1048576

commit v5 on v4

--- a/solution.py
+++ b/solution.py
@@ -134,7 +134,6 @@
             send(w_s.at[1 + part, core, rows], w_s.at[3, core, rows], s_w.at[4 + part], r_w.at[4 + part], to)
         )
 
-    weights_near(0)
     wides, nears, rest = [], [], []
     for r in range(1, 16):
         wides.append(send(part_s, wide_s.at[r], s_wide.at[r], r_wide.at[r], along_sp(r)))
@@ -145,6 +144,7 @@
     mods_s[tp] = total
     for k in range(1, 4):
         nears.append(send(mods_s.at[tp], mods_s.at[tp], s_near.at[k], r_near.at[k], along_tp(k)))
+    weights_near(0)
     for r in range(1, 16):
         rest.append(send(lat_hbm, clat_s.at[r], s_lat.at[r], r_lat.at[r], along_sp(r)))
         rest.append(send(rope_hbm, crope_s.at[r], s_rope.at[r], r_rope.at[r], along_sp(r)))
@@ -413,17 +413,18 @@
 
             lax.fori_loop(0, 3, some_tile, 0)
             prepare(chunk + 1)
-            step(chunk, 3, chunk + 1, 0)
+            step(chunk, 3, chunk + 1, 0 if chunk < 4 else 3)
         else:
-            for t in range(4):
-                step(chunk, t, chunk, t + 1 if t < 3 else None)
+            order = (3, 1, 2, 0)
+            for i, t in enumerate(order):
+                step(chunk, t, chunk, order[i + 1] if i < 3 else None)
                 finish(t)
-                if t:
-                    give(t - 1)
-            give(3)
+                if i:
+                    give(order[i - 1])
+            give(0)
 
     gate = [mods_s[i, j : j + 1, :] for i in range(4) for j in range(8, 12)]
-    for p in range(4):
+    for done, p in enumerate((3, 1, 2, 0)):
         k = OPPOSITE[p]
         for r in range(max(1, 4 * p), 4 * p + 4):
             att_copies[r].wait_recv()
@@ -433,9 +434,9 @@
         for n in range(4):
             cols = slice(512 * n, 512 * n + 512)
             term = dot(att, w_s[k, :, :, cols].reshape(256, 512)).astype(BF16).astype(F32)
-            if p:
+            if done:
                 term = mixed_s[:, cols] + term
-            if p < 3:
+            if done < 3:
                 mixed_s[:, cols] = term
             else:
                 gated = jnp.concatenate(gate[4 * n : 4 * n + 4], axis=1)

time: 63.5 us -> 63.7 us (level)
  no operation moved by 1% of the time
where the time goes in v5:
time: 63.7 us; the launch traced here: 63.5 us
  Pallas kernels  61.6 us (97%)
  local copies, waits for them, and re-layouts  1.88 us (3%)
    pallas_call x1, Pallas kernels, everything(): pl.pallas_call(kernel, out_shape=jax.ShapeDtypeStruct((128, 2048), BF16),...  61.6 us
    unnamed x1, local copies, waits for them, and re-layouts  1.88 us

profile of v5, /device:TPU:0, one launch (start us, length us, event | category | flops | bytes accessed | tf_op | source)
XLA Modules:
  0.0 63.5 jit_solution(9280815837845618641)
XLA Ops:
  0.0 61.6 %everything.1 = bf16[128,2048]{1,0:T(8,128)(2,1)} custom-call(bf16[1,128]{1,0:T(2,128)(2,1)} %bitcast.13, bf16[128,512]{1,0:T(8,128)(2,1)} %shift_hbm.1, bf16[128,512]{1,0:T(8,128)(2,1)} %scale_hbm.1, bf16[128,512]{1,0:T(8,128)(2,1)} %gate_hbm.1, f32[1,2048]{1,0:T(1,128)} %bitcast.9, f32[1,512]{1,0:T(1,128)} %bitcast.11, f32[1,256]{1,0:T(1,128)} %bitcast.12, ...), custom_call_target="tpu_custom_call" | custom-call | flops 10000000000 | bytes 8000000 | tf_op jit(solution)/shard_map/everything/pallas_call | solution.py:455
  61.7 1.9 %copy.22 = bf16[128,2048]{1,0:T(8,128)(2,1)} copy(bf16[128,2048]{1,0:T(8,128)(2,1)} %everything.1) | data formatting | bytes 1048576
